TPU v7x, 256 devices: a 4x2x16 block of a 4x16x16 slice. The times are simulated.
256 devices in a mesh: grp: 2 (over y), ep: 32 (over z, core), tp: 4 (over x).
Axes of the slice: x: 4, y: 2, z: 16, core: 2. Of those that a mesh axis runs over, the one named last changes fastest.
The devices are a block of a 4x16x16 slice.
Arguments:
- query_first: bfloat16 [24576, 512], P(('grp', 'ep'), 'tp'), parts along dimension 0, may hold values from -32 to 32
- query_second: bfloat16 [24576, 512], P(('grp', 'ep'), 'tp'), parts along dimension 0, may hold values from -32 to 32
- key_first: bfloat16 [24576, 512], P(('grp', 'ep'), 'tp'), parts along dimension 0, may hold values from -32 to 32
- key_second: bfloat16 [24576, 512], P(('grp', 'ep'), 'tp'), parts along dimension 0, may hold values from -32 to 32
- values: bfloat16 [24576, 1024], P(('grp', 'ep'), 'tp'), parts along dimension 0, may hold values from -6 to 6
- lambda_head: float32 [8], P('tp'), may hold values from 0.3 to 0.8
- head_gain: float32 [128], replicated, may hold values from 0.1 to 1.9
- out_weight: bfloat16 [1024, 2048], replicated, may hold values from -0.1875 to 0.1875
- tokens: bfloat16 [32768, 2048], P(('grp', 'ep', 'tp')), parts along dimension 0, may hold values from -6 to 6
- norm_gain: float32 [2048], replicated, may hold values from 0.1 to 1.9
- expert_ids: int32 [32768, 2], P(('grp', 'ep', 'tp')), parts along dimension 0, may hold values from 0 to 31, all different within a row; in each aligned block of 128 rows (0 to 127, 128 to 255, ...) at most 12 rows name the same one
- expert_weights: float32 [32768, 2], P(('grp', 'ep', 'tp')), parts along dimension 0, may hold values from 0.2 to 1
- expert_gate: bfloat16 [32, 2048, 1024], P('ep', None, 'tp'), may hold values from -0.125 to 0.125
- expert_up: bfloat16 [32, 2048, 1024], P('ep', None, 'tp'), may hold values from -0.125 to 0.125
- expert_down: bfloat16 [32, 1024, 2048], P('ep', 'tp'), may hold values from -0.1875 to 0.1875
- shared_gate: bfloat16 [2048, 512], P(None, 'tp'), may hold values from -0.125 to 0.125
- shared_up: bfloat16 [2048, 512], P(None, 'tp'), may hold values from -0.125 to 0.125
- shared_down: bfloat16 [512, 2048], P('tp'), may hold values from -0.25 to 0.25
Outputs:
- mixed: bfloat16 [24576, 2048], P(('grp', 'ep', 'tp')), parts along dimension 0
- expert_out: bfloat16 [32768, 2048], P(('grp', 'ep', 'tp')), parts along dimension 0
There are 2 independent parts, one for each index of `grp`. A program takes and returns all parts, laid end to end along the dimension named above; an argument that names none is the same for every part. Nothing has to cross between parts.
Inputs may be any that keep to these rules, and one draw needn't show every extreme that they name: `expert_ids`: in the rows of one device (aligned blocks of 128 rows) no expert is named by more than 12 rows, and in every draw some expert is named by exactly 12 rows of some block; each row names 2 different experts.
All inputs are finite; a program needn't handle non-finite values.
Results may differ from a plain program's by a relative error of at most 0.012.
Values may be sent and summed in bfloat16 or wider, within the bound.
A program may use at most 128 MiB of HBM per device.

v0:
```python
import jax
import jax.numpy as jnp
from jax import lax
from jax.sharding import Mesh
from jax.sharding import PartitionSpec as P

EP = ("ep_0", "ep_1")
GRP_EP = ("grp", "ep_0", "ep_1")
GRP_EP_TP = ("grp", "ep_0", "ep_1", "tp")


epsilon = 1e-06
block_limit = 1536


def sent_together(arrays, axis, dim, along):
    widths = [a.shape[along] for a in arrays]
    both = jnp.concatenate(arrays, axis=along)
    filled = lax.all_gather(both, axis, axis=dim, tiled=True)
    return tuple(jnp.split(filled, [sum(widths[:k]) for k in range(1, len(widths))], axis=along))


def in_blocks(value, dim, peers):
    before, after = (value.shape[:dim], value.shape[dim + 1 :])
    return jnp.moveaxis(value.reshape(*before, peers, -1, *after), dim, 0)


def in_order(tiles, dim):
    dims = list(tiles.shape[1:])
    dims[dim] *= tiles.shape[0]
    return jnp.moveaxis(tiles, 0, dim).reshape(dims)


def exchange_in_order(tiles, axes, order):
    dims = [lax.axis_size(a) for a in axes]
    tiles = tiles.reshape(*dims, *tiles.shape[1:])
    for k in order:
        tiles = lax.all_to_all(tiles, axes[k], split_axis=k, concat_axis=k, tiled=True)
    return tiles.reshape(-1, *tiles.shape[len(axes) :])


def two_step_exchange(value, groups, order, split_dim, concat_dim):
    peers = lax.axis_size(groups[0]) * lax.axis_size(groups[1])
    tiles = in_blocks(value, split_dim, peers)
    return in_order(exchange_in_order(tiles, groups, order), concat_dim)


def key_block(total_rows, shard_rows):
    best_rows = shard_rows
    for factor_rows in range(1, total_rows // shard_rows + 1):
        if total_rows % (factor_rows * shard_rows) == 0 and factor_rows * shard_rows <= block_limit:
            best_rows = factor_rows * shard_rows
    return best_rows


def softmax_update(states, scores, value_block):
    running_max, running_sum, accumulated = states
    new_max = jnp.maximum(running_max, jnp.max(scores, axis=-1))
    rescale = jnp.exp(running_max - new_max)
    weights = jnp.exp(scores - new_max[..., None])
    new_sum = running_sum * rescale + jnp.sum(weights, axis=-1)
    product = jnp.einsum(
        "qhk,khe->qhe",
        weights.astype(jnp.bfloat16),
        value_block,
        preferred_element_type=jnp.float32,
    )
    return (new_max, new_sum, accumulated * rescale[..., None] + product)


def shards(
    query_first,
    query_second,
    key_first,
    key_second,
    values,
    lambda_head,
    head_gain,
    out_weight,
    tokens,
    norm_gain,
    expert_ids,
    expert_weights,
    expert_gate,
    expert_up,
    expert_down,
    shared_gate,
    shared_up,
    shared_down,
):
    shard_rows, query_width = query_first.shape
    heads_here = lambda_head.shape[0]
    head_size = query_width // heads_here
    value_size = values.shape[1] // heads_here
    score_scale = head_size ** (-0.5)
    query_one = query_first.reshape(shard_rows, heads_here, head_size)
    query_two = query_second.reshape(shard_rows, heads_here, head_size)
    initial = (
        jnp.full((shard_rows, heads_here), -jnp.inf, jnp.float32),
        jnp.zeros((shard_rows, heads_here), jnp.float32),
        jnp.zeros((shard_rows, heads_here, value_size), jnp.float32),
    )
    carried = (initial, initial)
    key_one, key_two, value_piece = sent_together((key_first, key_second, values), EP, 0, 1)
    total_rows = key_one.shape[0]
    block_rows = key_block(total_rows, shard_rows)
    block_count = total_rows // block_rows
    stacked = (
        key_one.reshape(block_count, block_rows, heads_here, head_size),
        key_two.reshape(block_count, block_rows, heads_here, head_size),
        value_piece.reshape(block_count, block_rows, heads_here, value_size),
    )

    def fold_step(states, blocks):
        first_state, second_state = states
        key_a, key_b, value_block = blocks
        scores_a = (
            jnp.einsum("qhd,khd->qhk", query_one, key_a, preferred_element_type=jnp.float32)
            * score_scale
        )
        scores_b = (
            jnp.einsum("qhd,khd->qhk", query_two, key_b, preferred_element_type=jnp.float32)
            * score_scale
        )
        return (
            (
                softmax_update(first_state, scores_a, value_block),
                softmax_update(second_state, scores_b, value_block),
            ),
            None,
        )

    carried, unused = lax.scan(fold_step, carried, stacked)
    first_state, second_state = carried
    first_out = first_state[2] / first_state[1][..., None]
    second_out = second_state[2] / second_state[1][..., None]
    mixture = first_out - lambda_head[None, :, None] * second_out
    normed_heads = (
        mixture
        * lax.rsqrt(jnp.mean(mixture * mixture, axis=-1, keepdims=True) + epsilon)
        * head_gain
    )
    head_local = normed_heads.astype(jnp.bfloat16).reshape(shard_rows, heads_here * value_size)
    position_heads = lax.all_to_all(head_local, "tp", split_axis=0, concat_axis=1, tiled=True)
    mixed = jnp.dot(position_heads, out_weight, preferred_element_type=jnp.float32).astype(
        jnp.bfloat16
    )
    row_count, model_width = tokens.shape
    top_count = expert_ids.shape[1]
    ep_count = lax.axis_size(EP)
    local_experts = expert_gate.shape[0]
    expert_count = local_experts * ep_count
    capacity = max(2, row_count * top_count * 3 // (2 * expert_count))
    routed_rows = expert_count * capacity
    owner_span = routed_rows + row_count
    widened = tokens.astype(jnp.float32)
    normed = (
        widened
        * lax.rsqrt(jnp.mean(widened * widened, axis=-1, keepdims=True) + epsilon)
        * norm_gain
    ).astype(jnp.bfloat16)
    flat_ids = expert_ids.reshape(-1)
    onehot = (flat_ids[:, None] == jnp.arange(expert_count, dtype=jnp.int32)[None, :]).astype(
        jnp.int32
    )
    ranks = jnp.sum(onehot * jnp.cumsum(onehot, axis=0), axis=1) - 1
    slot_index = flat_ids * capacity + ranks
    token_index = jnp.arange(flat_ids.shape[0], dtype=jnp.int32) // top_count
    filled = jnp.full((routed_rows,), row_count, jnp.int32).at[slot_index].set(token_index)
    padded = jnp.concatenate([normed, jnp.zeros((1, model_width), jnp.bfloat16)], axis=0)
    outgoing = padded[filled].reshape(1, ep_count, local_experts * capacity, model_width)
    arrived = two_step_exchange(outgoing, ("ep_0", "ep_1"), (1, 0), 1, 1)
    local_rows = jnp.concatenate(
        [arrived.reshape(1, routed_rows, model_width), normed[None]], axis=1
    )
    gathered = lax.all_gather(local_rows, "tp", axis=0, tiled=True)
    owners = owner_span * lax.axis_size("tp") // owner_span
    routed_in = gathered[:, :routed_rows].reshape(
        owners, ep_count, local_experts, capacity, model_width
    )
    gate_value = jnp.einsum(
        "osecd,edf->osecf", routed_in, expert_gate, preferred_element_type=jnp.float32
    )
    up_value = jnp.einsum(
        "osecd,edf->osecf", routed_in, expert_up, preferred_element_type=jnp.float32
    )
    hidden = (jax.nn.silu(gate_value) * up_value).astype(jnp.bfloat16)
    routed_out = jnp.einsum(
        "osecf,efd->osecd", hidden, expert_down, preferred_element_type=jnp.float32
    )
    routed_out = routed_out.reshape(owners, routed_rows, model_width)
    shared_in = gathered[:, routed_rows:]
    shared_gate_value = jnp.einsum(
        "ord,df->orf", shared_in, shared_gate, preferred_element_type=jnp.float32
    )
    shared_up_value = jnp.einsum(
        "ord,df->orf", shared_in, shared_up, preferred_element_type=jnp.float32
    )
    shared_hidden = (jax.nn.silu(shared_gate_value) * shared_up_value).astype(jnp.bfloat16)
    shared_out = jnp.einsum(
        "orf,fd->ord", shared_hidden, shared_down, preferred_element_type=jnp.float32
    )
    kept_rows = lax.psum_scatter(
        jnp.concatenate([routed_out, shared_out], axis=1)
        .reshape(owners * owner_span, model_width)
        .astype(jnp.bfloat16),
        "tp",
        scatter_dimension=0,
        tiled=True,
    ).astype(jnp.float32)
    routed_back = (
        kept_rows[:routed_rows]
        .astype(jnp.bfloat16)
        .reshape(ep_count, local_experts * capacity, model_width)
    )
    returned = two_step_exchange(routed_back, ("ep_0", "ep_1"), (1, 0), 0, 0).reshape(
        routed_rows, model_width
    )
    picked = returned[slot_index].reshape(row_count, top_count, model_width).astype(jnp.float32)
    combined = jnp.sum(picked * expert_weights[:, :, None], axis=1) + kept_rows[routed_rows:]
    expert_out = combined.astype(jnp.bfloat16)
    return (mixed, expert_out)


def solution(mesh):
    torus = Mesh(
        mesh.devices.reshape(mesh.shape["grp"], 16, 2, mesh.shape["tp"]),
        ("grp", "ep_0", "ep_1", "tp"),
    )
    placed = (
        P(GRP_EP, "tp"),
        P(GRP_EP, "tp"),
        P(GRP_EP, "tp"),
        P(GRP_EP, "tp"),
        P(GRP_EP, "tp"),
        P("tp"),
        P(),
        P(),
        P(GRP_EP_TP, None),
        P(),
        P(GRP_EP_TP, None),
        P(GRP_EP_TP, None),
        P(EP, None, "tp"),
        P(EP, None, "tp"),
        P(EP, "tp", None),
        P(None, "tp"),
        P(None, "tp"),
        P("tp", None),
    )
    return jax.shard_map(
        shards,
        mesh=torus,
        in_specs=placed,
        out_specs=(P(GRP_EP_TP, None), P(GRP_EP_TP, None)),
        check_vma=False,
    )
```

profile of v0, /device:TPU:40, one launch (start us, length us, event | category | flops | bytes accessed | tf_op | source)
XLA Modules:
  0.0 628.7 jit_solution(13086468374661407831)
XLA Ops:
  14.2 3.1 gather_fusion
  17.3 2.4 reshape_transpose_reshape_reshape.3
  20.6 5.1 all_to_all.39
  25.7 2.8 copy.87
  28.5 24.0 %all-to-all-start.2 = ((bf16[16,2,1,1,12,2048]{5,1,4,3,2,0:T(2,128)(2,1)}), bf16[16,2,1,1,12,2048]{5,1,4,3,2,0:T(2,128)(2,1)}, u32[]{:S(2)}, u32[]{:S(2)}) async-start(bf16[16,2,1,1,12,2048]{5,1,4,3,2,0:T(2,128)(2,1)} %copy.87), calls=%async_computation.2 | async-start | bytes 3145728 | tf_op jit(solution)/shard_map/all_to_all | solution.py:38
  53.6 73.3 %all-to-all-done.2 = bf16[16,2,1,1,12,2048]{5,1,4,3,2,0:T(2,128)(2,1)} async-done(((bf16[16,2,1,1,12,2048]{5,1,4,3,2,0:T(2,128)(2,1)}), bf16[16,2,1,1,12,2048]{5,1,4,3,2,0:T(2,128)(2,1)}, u32[]{:S(2)}, u32[]{:S(2)}) %all-to-all-start.2) | async-done | bytes 1572896 | tf_op jit(solution)/shard_map/all_to_all | solution.py:38
  126.9 2.2 copy.88
  130.4 3.2 pad_maximum_fusion.1
  135.2 83.4 %all-gather.5.cloned.1.call-done = bf16[4,512,2048]{2,1,0:T(8,128)(2,1)} async-done(((bf16[1,512,2048]{2,1,0:T(8,128)(2,1)}), bf16[4,512,2048]{2,1,0:T(8,128)(2,1)}) %all-gather.5.cloned.1.call-update) | async-done | bytes 8388624 | tf_op jit(solution)/shard_map/all_gather | solution.py:176
  218.6 6.5 %slice.34 = bf16[4,384,2048]{2,1,0:T(8,128)(2,1)} slice(bf16[4,512,2048]{2,1,0:T(8,128)(2,1)} %all-gather.5.cloned.1.call-done), slice={[0:4], [0:384], [0:2048]} | slice | bytes 12582912 | tf_op jit(solution)/shard_map/slice | solution.py:178
  225.1 10.4 %copy.89 = bf16[4,384,2048]{2,0,1:T(4,128)(2,1)} copy(bf16[4,384,2048]{2,1,0:T(8,128)(2,1)} %slice.34) | data formatting | bytes 12582912 | tf_op jit(solution)/shard_map/slice | solution.py:178
  235.5 11.6 %fusion.44 = f32[4,32,12,256]{3,1,2,0:T(8,128)} fusion(bf16[4,32,12,2048]{3,0,2,1:T(4,128)(2,1)} %bitcast.191, bf16[1,2048,256]{2,1,0:T(8,128)(2,1)S(1)} %copy-done.15), kind=kOutput, calls=%fused_computation.52 | convolution fusion | flops 1610612736 | bytes 8912896 | tf_op jit(solution)/shard_map/osecd,edf->osecf/dot_general | solution.py:181
  247.2 17.0 %convert_bitcast_fusion = bf16[4,32,1,12,2048]{4,1,3,0,2:T(8,128)(2,1)} fusion(bf16[1,256,2048]{2,1,0:T(8,128)(2,1)S(1)} %copy-done, bf16[4,32,12,2048]{3,0,2,1:T(4,128)(2,1)} %bitcast.192, f32[4,32,12,256]{3,1,2,0:T(8,128)} %fusion.44, bf16[1,2048,256]{2,1,0:T(8,128)(2,1)} %param.33), kind=kOutput, calls=%fused_computation.49 | convolution fusion | flops 3226730496 | bytes 16252928 | tf_op jit(solution)/shard_map/osecf,efd->osecd/dot_general | solution.py:188
  264.2 10.5 %copy.92 = bf16[4,32,1,12,2048]{4,0,3,1,2:T(4,128)(2,1)} copy(bf16[4,32,1,12,2048]{4,1,3,0,2:T(8,128)(2,1)} %convert_bitcast_fusion) | data formatting | bytes 12582912 | tf_op jit(solution)/shard_map/osecf,efd->osecd/transpose | solution.py:188
  274.8 2.4 fusion.48
  277.1 5.3 convolution_convert_fusion
  282.4 3.2 copy.93
  285.7 8.4 %pad_maximum_fusion = bf16[4,512,2048]{2,0,1:T(4,128)(2,1)} fusion(bf16[4,128,2048]{2,0,1:T(4,128)(2,1)S(1)} %copy.93, bf16[4,384,2048]{2,0,1:T(4,128)(2,1)} %bitcast.190), kind=kLoop, calls=%fused_computation.48 | loop fusion | flops 4194304 | bytes 16777216 | tf_op jit(solution)/shard_map/concatenate | solution.py:204
  294.1 11.4 %copy.94 = bf16[4,512,2048]{2,1,0:T(8,128)(2,1)} copy(bf16[4,512,2048]{2,0,1:T(4,128)(2,1)} %pad_maximum_fusion) | data formatting | bytes 16777216 | tf_op jit(solution)/shard_map/concatenate | solution.py:204
  307.3 4.8 fusion.94
  312.1 11.6 %reshape.177 = bf16[8,1536,2,64]{3,2,1,0:T(2,128)(2,1)} reshape(bf16[12288,128]{1,0:T(8,128)(2,1)} %get-tuple-element.183) | data formatting | bytes 6291456 | tf_op jit(solution)/shard_map/reshape | solution.py:109
  323.8 15.5 %copy.77 = bf16[8,1536,2,64]{1,3,2,0:T(8,128)(2,1)} copy(bf16[8,1536,2,64]{3,2,1,0:T(2,128)(2,1)} %reshape.177) | data formatting | bytes 6291456
  339.2 11.6 %reshape.179 = bf16[8,1536,2,64]{3,2,1,0:T(2,128)(2,1)} reshape(bf16[12288,128]{1,0:T(8,128)(2,1)} %get-tuple-element.182) | data formatting | bytes 6291456 | tf_op jit(solution)/shard_map/reshape | solution.py:110
  350.9 15.6 %copy.79 = bf16[8,1536,2,64]{1,3,2,0:T(8,128)(2,1)} copy(bf16[8,1536,2,64]{3,2,1,0:T(2,128)(2,1)} %reshape.179) | data formatting | bytes 6291456
  366.4 6.4 %split.13 = bf16[12288,256]{1,0:T(8,128)(2,1)} slice(bf16[12288,512]{1,0:T(8,128)(2,1)} %all-gather.3.cloned.1.call-done), slice={[0:12288], [256:512]} | slice | bytes 12582912 | tf_op jit(solution)/shard_map/split | solution.py:20
  372.8 9.8 %reshape.178 = bf16[8,1536,2,128]{3,2,1,0:T(2,128)(2,1)} reshape(bf16[12288,256]{1,0:T(8,128)(2,1)} %split.13) | data formatting | bytes 12582912 | tf_op jit(solution)/shard_map/reshape | solution.py:111
  382.6 118.0 %while.21 = (s32[]{:T(128)}, f32[384,2]{0,1:T(2,128)S(1)}, f32[384,2]{0,1:T(2,128)S(1)}, f32[384,2,128]{0,2,1:T(8,128)S(1)}, f32[384,2]{0,1:T(2,128)S(1)}, /*ind...) while((s32[]{:T(128)}, f32[384,2]{0,1:T(2,128)S(1)}, ...), condition=%wide.region_5.6_spmd.clone, body=%wide.region_0.5_spmd.clone.sunk | while | flops 925441536 | bytes 92308720 | solution.py:133
  385.5 2.1 bitcast_reduce_fusion.5
  387.7 2.1 copy-done.4
  392.8 3.5 fusion.125
  400.3 2.1 bitcast_reduce_fusion.5
  402.5 2.1 copy-done.4
  407.6 3.5 fusion.125
  415.0 2.1 bitcast_reduce_fusion.5
  417.2 2.1 copy-done.4
  422.3 3.5 fusion.125
  429.8 2.1 bitcast_reduce_fusion.5
  431.9 2.1 copy-done.4
  437.0 3.5 fusion.125
  444.5 2.1 bitcast_reduce_fusion.5
  446.6 2.1 copy-done.4
  451.8 3.5 fusion.125
  459.2 2.1 bitcast_reduce_fusion.5
  461.4 2.1 copy-done.4
  466.5 3.5 fusion.125
  473.9 2.1 bitcast_reduce_fusion.5
  476.1 2.1 copy-done.4
  481.2 3.5 fusion.125
  488.6 2.1 bitcast_reduce_fusion.5
  490.8 2.1 copy-done.4
  495.9 3.5 fusion.125
  502.0 2.7 slice.36
  504.7 2.4 reshape_reshape_reshape.6
  508.0 5.0 all_to_all.40
  513.0 4.2 all-to-all-start
  517.2 2.8 copy.96
  520.0 3.6 all-to-all-done
  523.6 10.7 %all-to-all-start.4 = ((bf16[16,2,1,12,2048]{4,1,3,2,0:T(2,128)(2,1)}), bf16[16,2,1,12,2048]{4,1,3,2,0:T(2,128)(2,1)S(1)}, u32[]{:S(2)}, u32[]{:S(2)}) async-start(bf16[16,2,1,12,2048]{4,1,3,2,0:T(2,128)(2,1)} %copy.96), calls=%async_computation.5 | async-start | bytes 3145728 | tf_op jit(solution)/shard_map/all_to_all | solution.py:38
  534.4 3.7 convolution_convert_fusion.1
  538.2 69.0 %all-to-all-done.4 = bf16[16,2,1,12,2048]{4,1,3,2,0:T(2,128)(2,1)S(1)} async-done(((bf16[16,2,1,12,2048]{4,1,3,2,0:T(2,128)(2,1)}), bf16[16,2,1,12,2048]{4,1,3,2,0:T(2,128)(2,1)S(1)}, u32[]{:S(2)}, u32[]{:S(2)}) %all-to-all-start.4) | async-done | bytes 1572896 | tf_op jit(solution)/shard_map/all_to_all | solution.py:38
  609.3 2.5 reshape_reshape_reshape.7
  611.8 2.4 gather_fusion.1
  614.2 2.4 reshape.145
  616.5 3.2 multiply_reduce_fusion
  (213 shorter events, 75.1 us)
Async XLA Ops:
  7.2 240.0 %copy-start = (bf16[1,256,2048]{2,1,0:T(8,128)(2,1)S(1)}, bf16[1,256,2048]{2,1,0:T(8,128)(2,1)}, u32[]{:S(2)}) copy-start(bf16[1,256,2048]{2,1,0:T(8,128)(2,1)} %param.34) | copy-start | bytes 3145732
  20.6 32.0 %copy-start.5 = (bf16[128,2048]{1,0:T(8,128)(2,1)S(1)}, bf16[128,2048]{1,0:T(8,128)(2,1)}, u32[]{:S(2)}) copy-start(bf16[128,2048]{1,0:T(8,128)(2,1)} %param.28) | copy-start | bytes 1572868
  20.6 32.0 %copy-start.11 = (f32[2048]{0:T(1024)S(1)}, f32[2048]{0:T(1024)}, u32[]{:S(2)}) copy-start(f32[2048]{0:T(1024)} %param.29) | copy-start | bytes 24580
  28.5 98.3 %all-to-all-start.2 = ((bf16[16,2,1,1,12,2048]{5,1,4,3,2,0:T(2,128)(2,1)}), bf16[16,2,1,1,12,2048]{5,1,4,3,2,0:T(2,128)(2,1)}, u32[]{:S(2)}, u32[]{:S(2)}) async-start(bf16[16,2,1,1,12,2048]{5,1,4,3,2,0:T(2,128)(2,1)} %copy.87), calls=%async_computation.2 | async-start | bytes 3145728 | tf_op jit(solution)/shard_map/all_to_all | solution.py:38
  52.5 166.1 %all-gather.5.cloned.1.call-start = ((), (), s32[]{:S(2)}) async-start(), calls=%async_computation.7 | async-start | bytes 10485760 | tf_op jit(solution)/shard_map/all_gather | solution.py:176
  129.0 4.7 copy-start.6
  129.0 4.7 copy-start.7
  129.1 4.7 copy-start.8
  130.4 4.6 copy-start.9
  130.4 4.7 copy-start.10
  133.7 173.7 %all-gather.3.cloned.1.call-start = ((), (), s32[]{:S(2)}) async-start(), calls=%async_computation.6 | async-start | bytes 12976128 | tf_op jit(solution)/shard_map/all_gather | solution.py:19
  134.6 367.3 %reduce-scatter.2.cloned.1.call-start = ((), (), s32[]{:S(2)}) async-start(), calls=%async_computation.8 | async-start | bytes 10485760 | tf_op jit(solution)/shard_map/reduce_scatter | solution.py:203
  225.1 10.4 %copy-start.15 = (bf16[1,2048,256]{2,1,0:T(8,128)(2,1)S(1)}, bf16[1,2048,256]{2,1,0:T(8,128)(2,1)}, u32[]{:S(2)}) copy-start(bf16[1,2048,256]{2,1,0:T(8,128)(2,1)} %param.32) | copy-start | bytes 3145732
  264.2 10.5 %copy-start.16 = (bf16[2048,128]{1,0:T(8,128)(2,1)S(1)}, bf16[2048,128]{1,0:T(8,128)(2,1)}, u32[]{:S(2)}) copy-start(bf16[2048,128]{1,0:T(8,128)(2,1)} %param.35) | copy-start | bytes 1572868
  264.2 12.9 %copy-start.17 = (bf16[128,2048]{1,0:T(8,128)(2,1)S(1)}, bf16[128,2048]{1,0:T(8,128)(2,1)}, u32[]{:S(2)}) copy-start(bf16[128,2048]{1,0:T(8,128)(2,1)} %param.37) | copy-start | bytes 1572868
  264.2 12.9 %copy-start.18 = (bf16[2048,128]{1,0:T(8,128)(2,1)S(1)}, bf16[2048,128]{1,0:T(8,128)(2,1)}, u32[]{:S(2)}) copy-start(bf16[2048,128]{1,0:T(8,128)(2,1)} %param.36) | copy-start | bytes 1572868
  382.6 118.1 %copy-start.13 = (f32[2]{0:T(128)S(1)}, f32[2]{0:T(128)}, u32[]{:S(2)}) copy-start(f32[2]{0:T(128)} %param.25) | copy-start | bytes 28
  382.6 118.2 %copy-start.14 = (f32[128]{0:T(128)S(1)}, f32[128]{0:T(128)}, u32[]{:S(2)}) copy-start(f32[128]{0:T(128)} %param.26) | copy-start | bytes 1540
  384.7 3.0 copy-start.2
  387.7 2.1 copy-start.4
  392.8 3.8 copy-start.3
  399.5 2.9 copy-start.2
  402.4 2.1 copy-start.4
  407.6 3.8 copy-start.3
  414.2 2.9 copy-start.2
  417.2 2.1 copy-start.4
  422.3 3.8 copy-start.3
  428.9 2.9 copy-start.2
  431.9 2.1 copy-start.4
  437.0 3.8 copy-start.3
  443.7 2.9 copy-start.2
  446.6 2.1 copy-start.4
  451.8 3.8 copy-start.3
  458.4 2.9 copy-start.2
  461.3 2.1 copy-start.4
  466.5 3.8 copy-start.3
  473.1 2.9 copy-start.2
  476.1 2.1 copy-start.4
  481.2 3.8 copy-start.3
  487.8 2.9 copy-start.2
  490.8 2.1 copy-start.4
  495.9 3.8 copy-start.3
  508.0 26.3 %copy-start.12 = (f32[128,2]{0,1:T(2,128)S(1)}, f32[128,2]{0,1:T(2,128)}, u32[]{:S(2)}) copy-start(f32[128,2]{0,1:T(2,128)} %param.31) | copy-start | bytes 3076
  513.0 10.6 %all-to-all-start = ((bf16[4,96,256]{2,1,0:T(8,128)(2,1)}), bf16[4,96,256]{2,1,0:T(8,128)(2,1)S(1)}, u32[]{:S(2)}, u32[]{:S(2)}) async-start(bf16[4,96,256]{2,1,0:T(8,128)(2,1)} %all_to_all.26), calls=%async_computation | async-start | bytes 393216 | tf_op jit(solution)/shard_map/all_to_all | solution.py:144
  523.6 83.7 %all-to-all-start.4 = ((bf16[16,2,1,12,2048]{4,1,3,2,0:T(2,128)(2,1)}), bf16[16,2,1,12,2048]{4,1,3,2,0:T(2,128)(2,1)S(1)}, u32[]{:S(2)}, u32[]{:S(2)}) async-start(bf16[16,2,1,12,2048]{4,1,3,2,0:T(2,128)(2,1)} %copy.96), calls=%async_computation.5 | async-start | bytes 3145728 | tf_op jit(solution)/shard_map/all_to_all | solution.py:38
  611.8 9.9 %copy-start.1 = (bf16[1,256,2048]{2,1,0:T(8,128)(2,1)S(1)}, bf16[1,256,2048]{2,1,0:T(8,128)(2,1)}, u32[]{:S(2)}) copy-start(bf16[1,256,2048]{2,1,0:T(8,128)(2,1)} %param.34) | copy-start | bytes 3145732
Sparse Core Ops, SparseCore 0:
  133.8 84.7 all-gather.4
  221.0 86.2 all-gather.2
  310.0 83.3 reduce-scatter.1
where the time goes:
time: 638 us; the launch traced here: 629 us
  waiting for transfers between devices  231 us (36%)
  local copies, waits for them, and re-layouts  189 us (30%)
  matrix products  107 us (17%)
  starting transfers between devices  39.4 us (6%)
  other arithmetic  35.5 us (6%)
  between operations  14.7 us (2%)
  blocking collectives  10.2 us (2%)
    all_to_all x2, waiting for transfers between devices, exchange_in_order(): lax.all_to_all(tiles, axes[k], split_axis=k, concat_axis=k, tiled=True)  142 us
    all_gather x1, waiting for transfers between devices, shards(): gathered = lax.all_gather(local_rows, 'tp', axis=0, tiled=True)  83.4 us
    dot_general x16, matrix products, softmax_update(): jnp.einsum('qhk,khe->qhe', weights.astype(jnp.bfloat16), value_block, pre...  35.7 us
    all_to_all x2, starting transfers between devices, exchange_in_order(): lax.all_to_all(tiles, axes[k], split_axis=k, concat_axis=k, tiled=True)  34.7 us
    unnamed x38, local copies, waits for them, and re-layouts  32.3 us
    while x64, local copies, waits for them, and re-layouts  19.1 us
    dynamic_slice x16, local copies, waits for them, and re-layouts, shards(): carried, unused = lax.scan(fold_step, carried, stacked)  17.6 us
    dot_general x1, matrix products, shards(): jnp.einsum('osecf,efd->osecd', hidden, expert_down, preferred_element_typ...  17 us
  transfers between devices with their start and end apart: 6, of which 5 were waited for; matrix products, arithmetic and copies ran while one was open for 43% of the time, Pallas kernels for 0%

commit v1 on v0

v1 whole, which is shorter than its diff:
```python
import functools

import jax
import jax.numpy as jnp
from jax import lax
from jax.experimental import pallas as pl
from jax.experimental.pallas import tpu as pltpu
from jax.sharding import Mesh
from jax.sharding import PartitionSpec as P


EP = ("ep_0", "ep_1")
GRP_EP = ("grp", "ep_0", "ep_1")
GRP_EP_TP = ("grp", "ep_0", "ep_1", "tp")
LANES = 128
EPSILON = 1e-06


def contract(a, b, dims):
    return lax.dot_general(a, b, (dims, ((), ())), preferred_element_type=jnp.float32)


def attention_kernel(
    steps, head_size, lam_ref, gain_ref, q1_ref, q2_ref, kv_ref, out_ref, q_s, max_s, sum_s, acc_s
):
    step = pl.program_id(0)
    rows, q_width = q1_ref.shape
    heads = q_width // head_size
    value_size = out_ref.shape[1] // heads
    block = kv_ref.shape[0]

    @pl.when(step == 0)
    def _():
        lane_head = lax.broadcasted_iota(jnp.int32, (rows, q_width), 1) // head_size
        for m, q_ref in enumerate((q1_ref, q2_ref)):
            scaled = q_ref[...].astype(jnp.float32) * head_size ** (-0.5)
            for h in range(heads):
                q_s[m * heads + h] = jnp.where(lane_head == h, scaled, 0.0).astype(jnp.bfloat16)
        max_s[...] = jnp.full_like(max_s, -jnp.inf)
        sum_s[...] = jnp.zeros_like(sum_s)
        acc_s[...] = jnp.zeros_like(acc_s)

    for h in range(heads):
        value_from = 2 * q_width + h * value_size
        for m in range(2):
            i = m * heads + h
            scores = contract(q_s[i], kv_ref[:, m * q_width : (m + 1) * q_width], ((1,), (1,)))
            old_max = max_s[i]
            new_max = jnp.maximum(old_max, jnp.max(scores, axis=1, keepdims=True))
            rescale = jnp.exp(old_max - new_max)
            weights = jnp.exp(scores - new_max)
            lane_sum = weights[:, :LANES]
            for j in range(1, block // LANES):
                lane_sum = lane_sum + weights[:, j * LANES : (j + 1) * LANES]
            sum_s[i] = sum_s[i] * rescale + lane_sum
            product = contract(
                weights.astype(jnp.bfloat16),
                kv_ref[:, value_from : value_from + value_size],
                ((1,), (0,)),
            )
            acc_s[i] = acc_s[i] * rescale + product
            max_s[i] = new_max

    @pl.when(step == steps - 1)
    def _():
        for h in range(heads):
            first = acc_s[h] / jnp.sum(sum_s[h], axis=1, keepdims=True)
            second = acc_s[heads + h] / jnp.sum(sum_s[heads + h], axis=1, keepdims=True)
            mixture = first - lam_ref[h] * second
            power = jnp.mean(mixture * mixture, axis=1, keepdims=True)
            normed = mixture * lax.rsqrt(power + EPSILON) * gain_ref[...]
            out_ref[:, h * value_size : (h + 1) * value_size] = normed.astype(jnp.bfloat16)


def attention(q1, q2, kv, lam, gain):
    rows, q_width = q1.shape
    heads = lam.shape[0]
    value_width = heads * gain.shape[0]
    block = 3072
    steps = kv.shape[0] // block
    combos = 2 * heads
    flops = 2 * rows * kv.shape[0] * combos * (q_width // heads + gain.shape[0])
    return pl.pallas_call(
        functools.partial(attention_kernel, steps, q_width // heads),
        grid=(steps,),
        out_shape=jax.ShapeDtypeStruct((rows, value_width), jnp.bfloat16),
        in_specs=[
            pl.BlockSpec(memory_space=pltpu.SMEM),
            pl.BlockSpec((1, gain.shape[0]), lambda i: (0, 0)),
            pl.BlockSpec((rows, q_width), lambda i: (0, 0)),
            pl.BlockSpec((rows, q_width), lambda i: (0, 0)),
            pl.BlockSpec((block, kv.shape[1]), lambda i: (i, 0)),
        ],
        out_specs=pl.BlockSpec((rows, value_width), lambda i: (0, 0)),
        scratch_shapes=[
            pltpu.VMEM((combos, rows, q_width), jnp.bfloat16),
            pltpu.VMEM((combos, rows, 1), jnp.float32),
            pltpu.VMEM((combos, rows, LANES), jnp.float32),
            pltpu.VMEM((combos, rows, gain.shape[0]), jnp.float32),
        ],
        compiler_params=pltpu.CompilerParams(
            dimension_semantics=("arbitrary",), vmem_limit_bytes=48 * 2**20
        ),
        cost_estimate=pl.CostEstimate(
            flops=flops * 4, bytes_accessed=kv.size * 2, transcendentals=rows * kv.shape[0] * combos
        ),
        name="attention",
    )(lam, gain.reshape(1, -1), q1, q2, kv)


def ranked(ids):
    rows, top = ids.shape
    lower = lax.broadcasted_iota(jnp.int32, (rows, rows), 0) >= lax.broadcasted_iota(
        jnp.int32, (rows, rows), 1
    )
    lower = jnp.where(lower, 1.0, 0.0).astype(jnp.bfloat16)
    lane = lax.broadcasted_iota(jnp.int32, (rows, LANES), 1)
    before = jnp.zeros((1, LANES), jnp.float32)
    found = []
    for k in range(top):
        one = ids[:, k : k + 1] == lane
        ones = jnp.where(one, 1.0, 0.0)
        counts = contract(lower, ones.astype(jnp.bfloat16), ((1,), (0,))) + before
        rank = jnp.sum(jnp.where(one, counts, 0.0), axis=1, keepdims=True) - 1.0
        found.append((ids[:, k : k + 1], rank.astype(jnp.int32)))
        before = before + jnp.sum(ones, axis=0, keepdims=True)
    return found


def pack_kernel(
    capacity, core_ref, own_ref, other_ref, own_ids_ref, other_ids_ref, gain_ref,
    packed_ref, normed_ref,
):
    core = core_ref[0]
    slots = packed_ref.shape[0]
    rows = own_ref.shape[0]
    slot_lane = lax.broadcasted_iota(jnp.int32, (rows, slots), 1)
    masks, sources = [], []
    for ref, ids_ref, source in (
        (own_ref, own_ids_ref, core),
        (other_ref, other_ids_ref, 1 - core),
    ):
        wide = ref[...].astype(jnp.float32)
        power = jnp.mean(wide * wide, axis=1, keepdims=True)
        normed = (wide * lax.rsqrt(power + EPSILON) * gain_ref[...]).astype(jnp.bfloat16)
        if ref is own_ref:
            normed_ref[...] = normed
        hit = jnp.zeros((rows, slots), jnp.float32)
        for ids, rank in ranked(ids_ref[...]):
            slot = (ids >> 1) * (2 * capacity) + source * capacity + rank
            slot = jnp.where((ids & 1) == core, slot, -1)
            hit = hit + jnp.where(slot == slot_lane, 1.0, 0.0)
        masks.append(hit.astype(jnp.bfloat16))
        sources.append(normed)
    total = contract(masks[0], sources[0], ((0,), (0,)))
    total = total + contract(masks[1], sources[1], ((0,), (0,)))
    packed_ref[...] = total.astype(jnp.bfloat16)


def pack(core, own, other, own_ids, other_ids, gain, experts, capacity):
    rows, width = own.shape
    slots = experts * capacity
    vmem = pl.BlockSpec(memory_space=pltpu.VMEM)
    return pl.pallas_call(
        functools.partial(pack_kernel, capacity),
        out_shape=(
            jax.ShapeDtypeStruct((slots, width), jnp.bfloat16),
            jax.ShapeDtypeStruct((rows, width), jnp.bfloat16),
        ),
        in_specs=[pl.BlockSpec(memory_space=pltpu.SMEM)] + [vmem] * 5,
        out_specs=(vmem, vmem),
        compiler_params=pltpu.CompilerParams(vmem_limit_bytes=32 * 2**20),
        cost_estimate=pl.CostEstimate(
            flops=4 * slots * rows * width * 8, bytes_accessed=4 * rows * width * 2, transcendentals=0
        ),
        name="pack",
    )(core, own, other, own_ids, other_ids, gain.reshape(1, -1))


def silu_product(gate, up):
    return (gate / (1.0 + jnp.exp(-gate)) * up).astype(jnp.bfloat16)


def experts_kernel(width, gates, ups, downs, array_count, rows_ref, *refs):
    arrays = refs[:array_count]
    out_ref, gate_s, up_s, down_s, hidden_s, wide_sem, down_sem = refs[array_count:]
    parts = len(gates)

    def piece(where):
        return arrays[where[0]].at[where[1:]] if len(where) > 1 else arrays[where[0]]

    copies = []
    for p in range(parts):
        gate = pltpu.make_async_copy(piece(gates[p]), gate_s.at[p], wide_sem.at[0, p])
        up = pltpu.make_async_copy(piece(ups[p]), up_s.at[p], wide_sem.at[1, p])
        gate.start()
        up.start()
        copies.append((gate, up))
    downs_going = []
    at = 0
    for d, where in enumerate(downs):
        ref = piece(where)
        copy = pltpu.make_async_copy(ref, down_s.at[pl.ds(at, ref.shape[0])], down_sem.at[d])
        copy.start()
        downs_going.append(copy)
        at += ref.shape[0]
    for p in range(parts):
        copies[p][0].wait()
        gate = contract(rows_ref[...], gate_s[p], ((1,), (0,)))
        copies[p][1].wait()
        up = contract(rows_ref[...], up_s[p], ((1,), (0,)))
        hidden_s[:, p * width : (p + 1) * width] = silu_product(gate, up)
    for copy in downs_going:
        copy.wait()
    columns = out_ref.shape[1]
    tile = 512
    for c in range(columns // tile):
        piece = contract(hidden_s[...], down_s[:, c * tile : (c + 1) * tile], ((1,), (0,)))
        out_ref[:, c * tile : (c + 1) * tile] = piece.astype(out_ref.dtype)


def run_experts(rows, arrays, gates, ups, downs, width, out_dtype):
    parts = len(gates)
    hidden = parts * width
    model = rows.shape[1]
    hbm = pl.BlockSpec(memory_space=pltpu.MemorySpace.HBM)
    vmem = pl.BlockSpec(memory_space=pltpu.VMEM)
    return pl.pallas_call(
        functools.partial(experts_kernel, width, gates, ups, downs, len(arrays)),
        out_shape=jax.ShapeDtypeStruct(rows.shape, out_dtype),
        in_specs=[vmem] + [hbm] * len(arrays),
        out_specs=vmem,
        scratch_shapes=[
            pltpu.VMEM((parts, model, width), jnp.bfloat16),
            pltpu.VMEM((parts, model, width), jnp.bfloat16),
            pltpu.VMEM((hidden, model), jnp.bfloat16),
            pltpu.VMEM((rows.shape[0], hidden), jnp.bfloat16),
            pltpu.SemaphoreType.DMA((2, parts)),
            pltpu.SemaphoreType.DMA((len(downs),)),
        ],
        compiler_params=pltpu.CompilerParams(vmem_limit_bytes=61 * 2**20),
        cost_estimate=pl.CostEstimate(
            flops=6 * rows.shape[0] * model * hidden * 3,
            bytes_accessed=3 * hidden * model * 2,
            transcendentals=rows.shape[0] * hidden,
        ),
    )(rows, *arrays)


def combine_kernel(
    capacity, core_ref, own_ref, other_ref, ids_ref, weights_ref, shared_ref, out_ref
):
    core = core_ref[0]
    slots = own_ref.shape[0]
    rows = ids_ref.shape[0]
    slot_lane = lax.broadcasted_iota(jnp.int32, (rows, slots), 1)
    total = shared_ref[...]
    for k, (ids, rank) in enumerate(ranked(ids_ref[...])):
        slot = (ids >> 1) * (2 * capacity) + core * capacity + rank
        mine = (ids & 1) == core
        from_own = jnp.where(jnp.where(mine, slot, -1) == slot_lane, 1.0, 0.0)
        from_other = jnp.where(jnp.where(mine, -1, slot) == slot_lane, 1.0, 0.0)
        picked = contract(from_own.astype(jnp.bfloat16), own_ref[...], ((1,), (0,)))
        picked = picked + contract(from_other.astype(jnp.bfloat16), other_ref[...], ((1,), (0,)))
        total = total + weights_ref[:, k : k + 1] * picked
    out_ref[...] = total.astype(jnp.bfloat16)


def combine(core, own, other, ids, weights, shared, capacity):
    vmem = pl.BlockSpec(memory_space=pltpu.VMEM)
    return pl.pallas_call(
        functools.partial(combine_kernel, capacity),
        out_shape=jax.ShapeDtypeStruct(shared.shape, jnp.bfloat16),
        in_specs=[pl.BlockSpec(memory_space=pltpu.SMEM)] + [vmem] * 5,
        out_specs=vmem,
        compiler_params=pltpu.CompilerParams(vmem_limit_bytes=32 * 2**20),
        cost_estimate=pl.CostEstimate(
            flops=8 * own.size * ids.shape[0], bytes_accessed=own.size * 4, transcendentals=0
        ),
        name="combine",
    )(core, own, other, ids, weights, shared)


def shards(
    query_first,
    query_second,
    key_first,
    key_second,
    values,
    lambda_head,
    head_gain,
    out_weight,
    tokens,
    norm_gain,
    expert_ids,
    expert_weights,
    expert_gate,
    expert_up,
    expert_down,
    shared_gate,
    shared_up,
    shared_down,
):
    chips = lax.axis_size("ep_0")
    experts = expert_gate.shape[0] * lax.axis_size(EP)
    row_count, top_count = expert_ids.shape
    capacity = row_count * top_count * 3 // (2 * experts)
    width = tokens.shape[1]
    core = lax.axis_index("ep_1").reshape(1)
    ring = lax.axis_size("tp")
    to_right = [(i, (i + 1) % ring) for i in range(ring)]
    to_left = [(i, (i - 1) % ring) for i in range(ring)]

    def swap(value):
        return lax.ppermute(value, "ep_1", [(0, 1), (1, 0)])

    def right(value):
        return lax.ppermute(value, "tp", to_right)

    def left(value):
        return lax.ppermute(value, "tp", to_left)

    other_tokens = swap(tokens)
    other_ids = swap(expert_ids)

    gate, up, down = expert_gate[0], expert_up[0], expert_down[0]
    gate_l, up_r = right(gate), left(up)
    down_l, down_r = right(down), left(down)
    up_l, gate_r = right(up), left(gate)
    half = down.shape[0] // 2
    gate_o, up_o = right(gate_l), left(up_r)
    down_o1, down_o2 = right(down_l[:half]), left(down_r[half:])

    kv = lax.all_gather(
        jnp.concatenate([key_first, key_second, values], axis=1), EP, axis=0, tiled=True
    )

    packed, normed = pack(
        core, tokens, other_tokens, expert_ids, other_ids, norm_gain, experts, capacity
    )
    chunks = packed.reshape(chips, 2 * capacity, width)
    arrived = lax.all_to_all(chunks, "ep_0", split_axis=0, concat_axis=0, tiled=True)

    shared_both = jnp.concatenate([shared_gate, shared_up], axis=1)
    shared_both, shared_deep, gate_o, up_o, down_o1, down_o2 = lax.optimization_barrier(
        (shared_both, shared_down, gate_o, up_o, down_o1, down_o2)
    )
    shared_wide = lax.all_gather(shared_both, "tp", axis=0, tiled=False)
    shared_deep = lax.all_gather(shared_deep, "tp", axis=0, tiled=False)

    head_rows = attention(query_first, query_second, kv, lambda_head, head_gain)

    routed = run_experts(
        arrived.reshape(-1, width),
        (gate, gate_l, gate_r, gate_o, up, up_l, up_r, up_o)
        + (down, down_l, down_r, down_o1, down_o2),
        ((0,), (1,), (2,), (3,)),
        ((4,), (5,), (6,), (7,)),
        ((8,), (9,), (10,), (11,), (12,)),
        gate.shape[1],
        jnp.bfloat16,
    )
    outgoing = routed.reshape(chips, 2 * capacity, width)
    returned = lax.all_to_all(outgoing, "ep_0", split_axis=0, concat_axis=0, tiled=True)
    returned = returned.reshape(-1, width)

    part = shared_gate.shape[1]
    every = slice(None)
    shared = run_experts(
        normed,
        (shared_wide, shared_deep),
        tuple((0, i, every, pl.ds(0, part)) for i in range(ring)),
        tuple((0, i, every, pl.ds(part, part)) for i in range(ring)),
        tuple((1, i) for i in range(ring)),
        part,
        jnp.float32,
    )
    position_heads = lax.all_to_all(head_rows, "tp", split_axis=0, concat_axis=1, tiled=True)
    mixed = jnp.dot(position_heads, out_weight, preferred_element_type=jnp.float32).astype(
        jnp.bfloat16
    )
    expert_out = combine(
        core, returned, swap(returned), expert_ids, expert_weights, shared, capacity
    )
    return (mixed, expert_out)


def solution(mesh):
    torus = Mesh(
        mesh.devices.reshape(mesh.shape["grp"], mesh.shape["ep"] // 2, 2, mesh.shape["tp"]),
        ("grp", "ep_0", "ep_1", "tp"),
    )
    placed = (
        P(GRP_EP, "tp"),
        P(GRP_EP, "tp"),
        P(GRP_EP, "tp"),
        P(GRP_EP, "tp"),
        P(GRP_EP, "tp"),
        P("tp"),
        P(),
        P(),
        P(GRP_EP_TP, None),
        P(),
        P(GRP_EP_TP, None),
        P(GRP_EP_TP, None),
        P(EP, None, "tp"),
        P(EP, None, "tp"),
        P(EP, "tp", None),
        P(None, "tp"),
        P(None, "tp"),
        P("tp", None),
    )

    return jax.shard_map(
        shards,
        mesh=torus,
        in_specs=placed,
        out_specs=(P(GRP_EP_TP, None), P(GRP_EP_TP, None)),
        check_vma=False,
    )
```

time: 638 us -> 309 us (0.48); the launches traced: 629 us -> 307 us
  local copies, waits for them, and re-layouts: 189 us -> 6.72 us
  matrix products: 107 us -> 3.75 us
  waiting for transfers between devices: 231 us -> 161 us
  Pallas kernels: 0 us -> 58.9 us
  other arithmetic: 35.5 us -> 3.93 us
  starting transfers between devices: 39.4 us -> 58.7 us
  blocking collectives: 10.2 us -> 0 us
    dot_general x36 -> x0, matrix products: 104 us -> none  [the longest x16 35.7 us: softmax_update(): jnp.einsum('qhk,khe->qhe', weights.astype(jnp.bfloat16), value_block, pre...]
    ppermute x0 -> x13, waiting for transfers between devices: none -> 88.1 us  [the longest x5 43.7 us: right(): return lax.ppermute(value, 'tp', to_right)]
    all_gather x2 -> x3, waiting for transfers between devices: 85.1 us -> 0.04 us  [the longest x1 0.02 us: shards(): shared_deep = lax.all_gather(shared_deep, 'tp', axis=0, tiled=False)]
    all_to_all x3, waiting for transfers between devices: 146 us -> 72 us  [the longest x1 72 us: shards(): lax.all_to_all(outgoing, 'ep_0', split_axis=0, concat_axis=0, tiled=True)]
    pallas_call x0 -> x5, Pallas kernels: none -> 58.9 us  [the longest x1 32.9 us: attention(): pl.pallas_call(functools.partial(attention_kernel, steps, q_width // head...]
    reshape x3 -> x0, local copies, waits for them, and re-layouts: 33.1 us -> none  [the longest x1 11.6 us: shards(): key_one.reshape(block_count, block_rows, heads_here, head_size)]
    unnamed x38 -> x30, local copies, waits for them, and re-layouts: 32.3 us -> 6.63 us
    slice x4 -> x2, local copies, waits for them, and re-layouts: 19.8 us -> 0.07 us  [shards(): down_o1, down_o2 = (right(down_l[:half]), left(down_r[half:]))]
  transfers between devices with their start and end apart: 6 -> 19, of which waited for: 5 -> 6; matrix products, arithmetic and copies ran while one was open for 43% -> 1% of each run, Pallas kernels for 0% -> 19%
where the time goes in v1:
time: 309 us; the launch traced here: 307 us
  waiting for transfers between devices  161 us (52%)
  Pallas kernels  58.9 us (19%)
  starting transfers between devices  58.7 us (19%)
  between operations  14 us (5%)
  local copies, waits for them, and re-layouts  6.72 us (2%)
  other arithmetic  3.93 us (1%)
  matrix products  3.75 us (1%)
    all_to_all x1, waiting for transfers between devices, shards(): lax.all_to_all(outgoing, 'ep_0', split_axis=0, concat_axis=0, tiled=True)  72 us
    ppermute x5, waiting for transfers between devices, right(): return lax.ppermute(value, 'tp', to_right)  43.7 us
    ppermute x5, waiting for transfers between devices, left(): return lax.ppermute(value, 'tp', to_left)  43.5 us
    pallas_call x1, Pallas kernels, attention(): pl.pallas_call(functools.partial(attention_kernel, steps, q_width // head...  32.9 us
    all_to_all x1, starting transfers between devices, shards(): lax.all_to_all(chunks, 'ep_0', split_axis=0, concat_axis=0, tiled=True)  24.1 us
    pallas_call x2, Pallas kernels, run_experts(): pl.pallas_call(functools.partial(experts_kernel, width, gates, ups, downs...  19.4 us
    ppermute x5, starting transfers between devices, left(): return lax.ppermute(value, 'tp', to_left)  17.1 us
    all_to_all x1, starting transfers between devices, shards(): lax.all_to_all(outgoing, 'ep_0', split_axis=0, concat_axis=0, tiled=True)  11.8 us
  transfers between devices with their start and end apart: 19, of which 6 were waited for; matrix products, arithmetic and copies ran while one was open for 1% of the time, Pallas kernels for 19%

profile of v1, /device:TPU:40, one launch (start us, length us, event | category | flops | bytes accessed | tf_op | source)
XLA Modules:
  0.0 307.0 jit_solution(6236626457864899633)
XLA Ops:
  7.2 0.1 all-gather.6.cloned.1.call-start
  7.2 1.8 pad_maximum_fusion.1
  9.1 0.1 all-gather.6.cloned.1.call-update
  9.1 0.1 collective-permute-start
  9.3 0.8 copy.31.own_ids_ref.ids_ref
  10.1 0.6 collective-permute-start.1
  10.7 0.9 collective-permute-done.1.other_ids_ref
  11.6 0.0 collective-permute-done.other_ref
  11.6 1.0 copy-done.1
  12.6 0.7 copy-done.4
  13.3 2.7 pack.1
  16.0 0.8 copy-done.7
  16.8 24.1 %all-to-all-start.1 = ((bf16[16,24,2048]{2,1,0:T(8,128)(2,1)}), bf16[16,24,2048]{2,1,0:T(8,128)(2,1)S(1)}, u32[]{:S(2)}, u32[]{:S(2)}) async-start(bf16[16,24,2048]{2,1,0:T(8,128)(2,1)} %bitcast.5), calls=%async_computation.1 | async-start | bytes 3145728 | tf_op jit(solution)/shard_map/all_to_all | solution.py:342
  40.9 0.1 all-gather.10.cloned.1.call-start
  41.0 3.3 %collective-permute-start.9 = (bf16[256,2048]{1,0:T(8,128)(2,1)}, bf16[256,2048]{1,0:T(8,128)(2,1)S(1)}, u32[]{:S(2)}, u32[]{:S(2)}) collective-permute-start(bf16[256,2048]{1,0:T(8,128)(2,1)} %bitcast.34), channel_id=1, source_target_pairs={{0,3},{1,0},{2,1},{3,2},{4,7},{5,4},{6,5},{7,6},{8,11},{9,8},{10,9... | collective-permute-start | bytes 3145736 | tf_op jit(solution)/shard_map/ppermute | solution.py:321
  44.3 0.0 collective-permute-start.2
  44.3 3.2 %collective-permute-start.5 = (bf16[2048,256]{1,0:T(8,128)(2,1)}, bf16[2048,256]{1,0:T(8,128)(2,1)}, u32[]{:S(2)}, u32[]{:S(2)}) collective-permute-start(bf16[2048,256]{1,0:T(8,128)(2,1)} %bitcast.31), channel_id=1, source_target_pairs={{0,3},{1,0},{2,1},{3,2},{4,7},{5,4},{6,5},{7,6},{8,11},{9,8},{10,9... | collective-permute-start | bytes 3145736 | tf_op jit(solution)/shard_map/ppermute | solution.py:321
  47.5 0.0 collective-permute-start.7
  47.5 20.6 %collective-permute-done.9.refs_10_ = bf16[256,2048]{1,0:T(8,128)(2,1)S(1)} collective-permute-done((bf16[256,2048]{1,0:T(8,128)(2,1)}, bf16[256,2048]{1,0:T(8,128)(2,1)S(1)}, u32[]{:S(2)}, u32[]{:S(2)}) %collective-permute-start.9) | collective-permute-done | bytes 1048608 | tf_op jit(solution)/shard_map/ppermute | solution.py:321
  68.2 3.7 %collective-permute-start.10 = (bf16[128,2048]{1,0:T(8,128)(2,1)S(1)}, bf16[128,2048]{1,0:T(8,128)(2,1)S(1)}, u32[]{:S(2)}, u32[]{:S(2)}) collective-permute-start(bf16[128,2048]{1,0:T(8,128)(2,1)S(1)} %slice.9), channel_id=1, source_target_pairs={{0,3},{1,0},{2,1},{3,2},{4,7},{5,4},{6,5},{7,6},{8,11},{9,8},{10,9... | collective-permute-start | bytes 1572872 | tf_op jit(solution)/shard_map/ppermute | solution.py:321
  71.9 0.0 collective-permute-done.2.refs_1_
  71.9 0.0 collective-permute-start.4
  71.9 18.7 %collective-permute-done.5.refs_6_ = bf16[2048,256]{1,0:T(8,128)(2,1)} collective-permute-done((bf16[2048,256]{1,0:T(8,128)(2,1)}, bf16[2048,256]{1,0:T(8,128)(2,1)}, u32[]{:S(2)}, u32[]{:S(2)}) %collective-permute-start.5) | collective-permute-done | bytes 1048608 | tf_op jit(solution)/shard_map/ppermute | solution.py:321
  90.6 3.7 %collective-permute-start.6 = (bf16[2048,256]{1,0:T(8,128)(2,1)}, bf16[2048,256]{1,0:T(8,128)(2,1)}, u32[]{:S(2)}, u32[]{:S(2)}) collective-permute-start(bf16[2048,256]{1,0:T(8,128)(2,1)} %collective-permute-done.5.refs_6_), channel_id=1, source_target_pairs={{0,3},{1,0},{2,1},{3,2},{4,7},{5,4},{6,5},{7,6},{8,11},{9,8},{10,9... | collective-permute-start | bytes 3145736 | tf_op jit(solution)/shard_map/ppermute | solution.py:321
  94.3 0.0 collective-permute-start.11
  94.3 0.0 collective-permute-done.7.refs_9_
  94.3 3.2 %collective-permute-start.3 = (bf16[2048,256]{1,0:T(8,128)(2,1)}, bf16[2048,256]{1,0:T(8,128)(2,1)}, u32[]{:S(2)}, u32[]{:S(2)}) collective-permute-start(bf16[2048,256]{1,0:T(8,128)(2,1)} %bitcast.29), channel_id=1, source_target_pairs={{0,3},{1,0},{2,1},{3,2},{4,7},{5,4},{6,5},{7,6},{8,11},{9,8},{10,9... | collective-permute-start | bytes 3145736 | tf_op jit(solution)/shard_map/ppermute | solution.py:321
  97.6 4.2 %collective-permute-done.10.refs_12_ = bf16[128,2048]{1,0:T(8,128)(2,1)S(1)} collective-permute-done((bf16[128,2048]{1,0:T(8,128)(2,1)S(1)}, bf16[128,2048]{1,0:T(8,128)(2,1)S(1)}, u32[]{:S(2)}, u32[]{:S(2)}) %collective-permute-start.10) | collective-permute-done | bytes 524320 | tf_op jit(solution)/shard_map/ppermute | solution.py:321
  101.7 0.8 copy-done.13
  102.5 0.9 collective-permute-start.8
  103.5 2.1 pad_maximum_fusion
  105.6 43.7 %collective-permute-done.8.refs_11_ = bf16[128,2048]{1,0:T(8,128)(2,1)} collective-permute-done((bf16[128,2048]{1,0:T(8,128)(2,1)S(1)}, bf16[128,2048]{1,0:T(8,128)(2,1)}, u32[]{:S(2)}, u32[]{:S(2)}) %collective-permute-start.8) | collective-permute-done | bytes 524320 | tf_op jit(solution)/shard_map/ppermute | solution.py:318
  149.3 0.0 collective-permute-done.4.refs_3_
  149.3 0.0 collective-permute-done.6.refs_7_
  149.3 0.1 all-gather.10.cloned.1.call-update
  149.4 0.0 collective-permute-done.11.refs_5_
  149.4 0.0 collective-permute-done.3.refs_2_
  149.4 0.0 all-to-all-done.1
  149.4 1.2 copy-done.8
  150.6 13.5 %shard_map.185 = bf16[384,2048]{1,0:T(8,128)(2,1)} custom-call(bf16[384,2048]{1,0:T(8,128)(2,1)} %bitcast.22, bf16[2048,256]{1,0:T(8,128)(2,1)} %bitcast.30, bf16[2048,256]{1,0:T(8,128)(2,1)} %collective-permute-done.2.refs_1_, bf16[2048,256]{1,0:T(8,128)(2,1)} %collective-permute-done.3.refs_2_, bf16[2048,256]{1,0:T(8,128)(2,1)} %collective-permute-done.4.refs_3_, ...), custom_call_target="tpu_custom_call" | custom-call | flops 14495514624 | bytes 12582912 | tf_op jit(solution)/shard_map/pallas_call | solution.py:228
  164.0 0.0 copy-start.12
  164.1 0.0 copy-start.2
  164.1 0.0 copy-start.3
  164.1 0.0 copy-start.5
  164.1 0.0 copy-start.6
  164.1 11.8 %all-to-all-start.2 = ((bf16[16,24,2048]{2,1,0:T(8,128)(2,1)}), bf16[16,24,2048]{2,1,0:T(8,128)(2,1)S(1)}, u32[]{:S(2)}, u32[]{:S(2)}) async-start(bf16[16,24,2048]{2,1,0:T(8,128)(2,1)} %bitcast.23), calls=%async_computation.2 | async-start | bytes 3145728 | tf_op jit(solution)/shard_map/all_to_all | solution.py:364
  175.9 0.1 all-gather.8.cloned.1.call-start
  176.0 0.7 all-gather.8.cloned.1.call-update
  176.8 0.1 copy.33.weights_ref
  176.9 72.0 %all-to-all-done.2 = bf16[16,24,2048]{2,1,0:T(8,128)(2,1)S(1)} async-done(((bf16[16,24,2048]{2,1,0:T(8,128)(2,1)}), bf16[16,24,2048]{2,1,0:T(8,128)(2,1)S(1)}, u32[]{:S(2)}, u32[]{:S(2)}) %all-to-all-start.2) | async-done | bytes 1572896 | tf_op jit(solution)/shard_map/all_to_all | solution.py:364
  248.9 0.0 collective-permute-start.12
  248.9 0.0 copy-done.2
  248.9 0.0 copy-done.3
  248.9 0.0 copy-done.5
  248.9 32.9 %attention.1 = bf16[384,256]{1,0:T(8,128)(2,1)} custom-call(f32[2]{0:T(128)S(1)} %copy-done.5, f32[1,128]{1,0:T(1,128)S(1)} %bitcast.21, bf16[384,128]{1,0:T(8,128)(2,1)S(1)} %copy-done.2, bf16[384,128]{1,0:T(8,128)(2,1)S(1)} %copy-done.3, bf16[12288,512]{1,0:T(8,128)(2,1)} %all-gather.6.cloned.1.call-done.kv_ref), custom_call_target="tpu_custom_call" | custom-call | flops 28991029248 | bytes 12582912 | tf_op jit(solution)/shard_map/attention/pallas_call | solution.py:83
  281.9 3.7 %all-to-all-start = ((bf16[4,96,256]{2,1,0:T(8,128)(2,1)}), bf16[4,96,256]{2,1,0:T(8,128)(2,1)S(1)}, u32[]{:S(2)}, u32[]{:S(2)}) async-start(bf16[4,96,256]{2,1,0:T(8,128)(2,1)} %bitcast.1), calls=%async_computation | async-start | bytes 393216 | tf_op jit(solution)/shard_map/all_to_all | solution.py:378
  285.6 0.0 all-gather.10.cloned.1.call-done
  285.6 0.0 all-gather.8.cloned.1.call-done
  285.7 6.0 %shard_map.186.shared_ref = f32[128,2048]{1,0:T(8,128)} custom-call(bf16[128,2048]{1,0:T(8,128)(2,1)} %copy-done.7, bf16[4,2048,256]{2,1,0:T(8,128)(2,1)} %bitcast.26, bf16[4,128,2048]{2,1,0:T(8,128)(2,1)} %bitcast.27), custom_call_target="tpu_custom_call" | custom-call | flops 2415919104 | bytes 6291456 | tf_op jit(solution)/shard_map/pallas_call | solution.py:228
  291.6 0.0 collective-permute-done.12.other_ref
  291.6 1.2 copy-done
  292.9 3.8 %combine.1 = bf16[128,2048]{1,0:T(8,128)(2,1)} custom-call(s32[1]{0:T(128)} %bitcast.3.core_ref, bf16[384,2048]{1,0:T(8,128)(2,1)S(1)} %bitcast.19, bf16[384,2048]{1,0:T(8,128)(2,1)} %collective-permute-done.12.other_ref, s32[128,2]{1,0:T(8,128)S(1)} %copy.31.own_ids_ref.ids_ref, f32[128,2]{1,0:T(8,128)S(1)} %copy.33.weights_ref, f32[128,2048]{1,0:T(8,128)S(1)} %copy-done), custom_call_target="tpu_custom_call" | custom-call | flops 805306368 | bytes 3145728 | tf_op jit(solution)/shard_map/combine/pallas_call | solution.py:271
  296.7 0.0 all-to-all-done
  296.7 3.8 %convolution_convert_fusion = bf16[96,2048]{1,0:T(8,128)(2,1)} fusion(bf16[96,1024]{1,0:T(8,128)(2,1)S(1)} %bitcast.24, bf16[1024,2048]{1,0:T(8,128)(2,1)} %param.25), kind=kOutput, calls=%fused_computation | convolution fusion | flops 402849792 | bytes 4784128 | tf_op jit(solution)/shard_map/dot_general | solution.py:379
  (18 shorter events, 0.1 us)
Async XLA Ops:
  7.2 241.7 %all-gather.6.cloned.1.call-start = ((), (), s32[]{:S(2)}) async-start(), calls=%async_computation.3 | async-start | bytes 12976128 | tf_op jit(solution)/shard_map/all_gather | solution.py:334
  9.1 2.4 collective-permute-start
  10.1 1.5 collective-permute-start.1
  11.6 1.0 copy-start.1
  12.6 0.7 copy-start.4
  16.0 0.8 copy-start.7
  16.8 86.7 %copy-start.9 = (bf16[2048,128]{1,0:T(8,128)(2,1)S(1)}, bf16[2048,128]{1,0:T(8,128)(2,1)}, u32[]{:S(2)}) copy-start(bf16[2048,128]{1,0:T(8,128)(2,1)} %param.34) | copy-start | bytes 1572868
  16.8 132.6 %all-to-all-start.1 = ((bf16[16,24,2048]{2,1,0:T(8,128)(2,1)}), bf16[16,24,2048]{2,1,0:T(8,128)(2,1)S(1)}, u32[]{:S(2)}, u32[]{:S(2)}) async-start(bf16[16,24,2048]{2,1,0:T(8,128)(2,1)} %bitcast.5), calls=%async_computation.1 | async-start | bytes 3145728 | tf_op jit(solution)/shard_map/all_to_all | solution.py:342
  40.9 244.7 %all-gather.10.cloned.1.call-start = ((), (), s32[]{:S(2)}) async-start(), calls=%async_computation.5 | async-start | bytes 2621440 | tf_op jit(solution)/shard_map/all_gather | solution.py:349
  41.0 27.1 %collective-permute-start.9 = (bf16[256,2048]{1,0:T(8,128)(2,1)}, bf16[256,2048]{1,0:T(8,128)(2,1)S(1)}, u32[]{:S(2)}, u32[]{:S(2)}) collective-permute-start(bf16[256,2048]{1,0:T(8,128)(2,1)} %bitcast.34), channel_id=1, source_target_pairs={{0,3},{1,0},{2,1},{3,2},{4,7},{5,4},{6,5},{7,6},{8,11},{9,8},{10,9... | collective-permute-start | bytes 3145736 | tf_op jit(solution)/shard_map/ppermute | solution.py:321
  44.3 27.6 %collective-permute-start.2 = (bf16[2048,256]{1,0:T(8,128)(2,1)}, bf16[2048,256]{1,0:T(8,128)(2,1)}, u32[]{:S(2)}, u32[]{:S(2)}) collective-permute-start(bf16[2048,256]{1,0:T(8,128)(2,1)} %bitcast.28), channel_id=1, source_target_pairs={{0,1},{1,2},{2,3},{3,0},{4,5},{5,6},{6,7},{7,4},{8,9},{9,10},{10,1... | collective-permute-start | bytes 3145736 | tf_op jit(solution)/shard_map/ppermute | solution.py:318
  44.3 46.3 %collective-permute-start.5 = (bf16[2048,256]{1,0:T(8,128)(2,1)}, bf16[2048,256]{1,0:T(8,128)(2,1)}, u32[]{:S(2)}, u32[]{:S(2)}) collective-permute-start(bf16[2048,256]{1,0:T(8,128)(2,1)} %bitcast.31), channel_id=1, source_target_pairs={{0,3},{1,0},{2,1},{3,2},{4,7},{5,4},{6,5},{7,6},{8,11},{9,8},{10,9... | collective-permute-start | bytes 3145736 | tf_op jit(solution)/shard_map/ppermute | solution.py:321
  47.5 46.8 %collective-permute-start.7 = (bf16[256,2048]{1,0:T(8,128)(2,1)}, bf16[256,2048]{1,0:T(8,128)(2,1)S(1)}, u32[]{:S(2)}, u32[]{:S(2)}) collective-permute-start(bf16[256,2048]{1,0:T(8,128)(2,1)} %bitcast.35), channel_id=1, source_target_pairs={{0,1},{1,2},{2,3},{3,0},{4,5},{5,6},{6,7},{7,4},{8,9},{9,10},{10,1... | collective-permute-start | bytes 3145736 | tf_op jit(solution)/shard_map/ppermute | solution.py:318
  68.1 33.6 %copy-start.10 = (bf16[256,2048]{1,0:T(8,128)(2,1)}, bf16[256,2048]{1,0:T(8,128)(2,1)S(1)}, u32[]{:S(2)}) copy-start(bf16[256,2048]{1,0:T(8,128)(2,1)S(1)} %collective-permute-done.9.refs_10_) | copy-start | bytes 3145732
  68.2 33.6 %collective-permute-start.10 = (bf16[128,2048]{1,0:T(8,128)(2,1)S(1)}, bf16[128,2048]{1,0:T(8,128)(2,1)S(1)}, u32[]{:S(2)}, u32[]{:S(2)}) collective-permute-start(bf16[128,2048]{1,0:T(8,128)(2,1)S(1)} %slice.9), channel_id=1, source_target_pairs={{0,3},{1,0},{2,1},{3,2},{4,7},{5,4},{6,5},{7,6},{8,11},{9,8},{10,9... | collective-permute-start | bytes 1572872 | tf_op jit(solution)/shard_map/ppermute | solution.py:321
  71.9 77.4 %collective-permute-start.4 = (bf16[2048,256]{1,0:T(8,128)(2,1)}, bf16[2048,256]{1,0:T(8,128)(2,1)}, u32[]{:S(2)}, u32[]{:S(2)}) collective-permute-start(bf16[2048,256]{1,0:T(8,128)(2,1)} %collective-permute-done.2.refs_1_), channel_id=1, source_target_pairs={{0,1},{1,2},{2,3},{3,0},{4,5},{5,6},{6,7},{7,4},{8,9},{9,10},{10,1... | collective-permute-start | bytes 3145736 | tf_op jit(solution)/shard_map/ppermute | solution.py:318
  90.6 58.7 %collective-permute-start.6 = (bf16[2048,256]{1,0:T(8,128)(2,1)}, bf16[2048,256]{1,0:T(8,128)(2,1)}, u32[]{:S(2)}, u32[]{:S(2)}) collective-permute-start(bf16[2048,256]{1,0:T(8,128)(2,1)} %collective-permute-done.5.refs_6_), channel_id=1, source_target_pairs={{0,3},{1,0},{2,1},{3,2},{4,7},{5,4},{6,5},{7,6},{8,11},{9,8},{10,9... | collective-permute-start | bytes 3145736 | tf_op jit(solution)/shard_map/ppermute | solution.py:321
  94.3 55.1 %collective-permute-start.11 = (bf16[2048,256]{1,0:T(8,128)(2,1)}, bf16[2048,256]{1,0:T(8,128)(2,1)}, u32[]{:S(2)}, u32[]{:S(2)}) collective-permute-start(bf16[2048,256]{1,0:T(8,128)(2,1)} %bitcast.32), channel_id=1, source_target_pairs={{0,1},{1,2},{2,3},{3,0},{4,5},{5,6},{6,7},{7,4},{8,9},{9,10},{10,1... | collective-permute-start | bytes 3145736 | tf_op jit(solution)/shard_map/ppermute | solution.py:318
  94.3 7.4 %copy-start.11 = (bf16[256,2048]{1,0:T(8,128)(2,1)}, bf16[256,2048]{1,0:T(8,128)(2,1)S(1)}, u32[]{:S(2)}) copy-start(bf16[256,2048]{1,0:T(8,128)(2,1)S(1)} %collective-permute-done.7.refs_9_) | copy-start | bytes 3145732
  94.3 55.1 %collective-permute-start.3 = (bf16[2048,256]{1,0:T(8,128)(2,1)}, bf16[2048,256]{1,0:T(8,128)(2,1)}, u32[]{:S(2)}, u32[]{:S(2)}) collective-permute-start(bf16[2048,256]{1,0:T(8,128)(2,1)} %bitcast.29), channel_id=1, source_target_pairs={{0,3},{1,0},{2,1},{3,2},{4,7},{5,4},{6,5},{7,6},{8,11},{9,8},{10,9... | collective-permute-start | bytes 3145736 | tf_op jit(solution)/shard_map/ppermute | solution.py:321
  101.7 0.8 copy-start.13
  102.5 46.8 %collective-permute-start.8 = (bf16[128,2048]{1,0:T(8,128)(2,1)S(1)}, bf16[128,2048]{1,0:T(8,128)(2,1)}, u32[]{:S(2)}, u32[]{:S(2)}) collective-permute-start(bf16[128,2048]{1,0:T(8,128)(2,1)S(1)} %slice.8), channel_id=1, source_target_pairs={{0,1},{1,2},{2,3},{3,0},{4,5},{5,6},{6,7},{7,4},{8,9},{9,10},{10,1... | collective-permute-start | bytes 1572872 | tf_op jit(solution)/shard_map/ppermute | solution.py:318
  149.4 1.2 copy-start.8
  164.0 12.7 %copy-start.12 = (f32[128,2]{0,1:T(2,128)S(1)}, f32[128,2]{0,1:T(2,128)}, u32[]{:S(2)}) copy-start(f32[128,2]{0,1:T(2,128)} %param.29) | copy-start | bytes 3076
  164.1 84.9 %copy-start.2 = (bf16[384,128]{1,0:T(8,128)(2,1)S(1)}, bf16[384,128]{1,0:T(8,128)(2,1)}, u32[]{:S(2)}) copy-start(bf16[384,128]{1,0:T(8,128)(2,1)} %q1_ref.1) | copy-start | bytes 294916
  164.1 84.9 %copy-start.3 = (bf16[384,128]{1,0:T(8,128)(2,1)S(1)}, bf16[384,128]{1,0:T(8,128)(2,1)}, u32[]{:S(2)}) copy-start(bf16[384,128]{1,0:T(8,128)(2,1)} %q2_ref.1) | copy-start | bytes 294916
  164.1 84.8 %copy-start.5 = (f32[2]{0:T(128)S(1)}, f32[2]{0:T(128)}, u32[]{:S(2)}) copy-start(f32[2]{0:T(128)} %lam_ref.1) | copy-start | bytes 28
  164.1 84.8 %copy-start.6 = (f32[128]{0:T(128)S(1)}, f32[128]{0:T(128)}, u32[]{:S(2)}) copy-start(f32[128]{0:T(128)} %param.24) | copy-start | bytes 1540
  164.1 84.8 %all-to-all-start.2 = ((bf16[16,24,2048]{2,1,0:T(8,128)(2,1)}), bf16[16,24,2048]{2,1,0:T(8,128)(2,1)S(1)}, u32[]{:S(2)}, u32[]{:S(2)}) async-start(bf16[16,24,2048]{2,1,0:T(8,128)(2,1)} %bitcast.23), calls=%async_computation.2 | async-start | bytes 3145728 | tf_op jit(solution)/shard_map/all_to_all | solution.py:364
  175.9 109.7 %all-gather.8.cloned.1.call-start = ((), (), s32[]{:S(2)}) async-start(), calls=%async_computation.4 | async-start | bytes 5242880 | tf_op jit(solution)/shard_map/all_gather | solution.py:348
  248.9 42.7 %collective-permute-start.12 = (bf16[384,2048]{1,0:T(8,128)(2,1)S(1)}, bf16[384,2048]{1,0:T(8,128)(2,1)}, u32[]{:S(2)}, u32[]{:S(2)}) collective-permute-start(bf16[384,2048]{1,0:T(8,128)(2,1)S(1)} %bitcast.18), channel_id=1, source_target_pairs={{0,4},{4,0},{1,5},{5,1},{2,6},{6,2},{3,7},{7,3},{8,12},{12,8},{9,1... | collective-permute-start | bytes 4718600 | tf_op jit(solution)/shard_map/ppermute | solution.py:315
  281.9 14.8 %all-to-all-start = ((bf16[4,96,256]{2,1,0:T(8,128)(2,1)}), bf16[4,96,256]{2,1,0:T(8,128)(2,1)S(1)}, u32[]{:S(2)}, u32[]{:S(2)}) async-start(bf16[4,96,256]{2,1,0:T(8,128)(2,1)} %bitcast.1), calls=%async_computation | async-start | bytes 393216 | tf_op jit(solution)/shard_map/all_to_all | solution.py:378
  291.6 1.2 copy-start
Sparse Core Ops, SparseCore 0:
  10.4 165.9 all-gather.5
  178.2 41.3 all-gather.9
  221.5 54.3 all-gather.7

commit v2 on v1

--- a/solution.py
+++ b/solution.py
@@ -341,12 +341,9 @@
     chunks = packed.reshape(chips, 2 * capacity, width)
     arrived = lax.all_to_all(chunks, "ep_0", split_axis=0, concat_axis=0, tiled=True)
 
-    shared_both = jnp.concatenate([shared_gate, shared_up], axis=1)
-    shared_both, shared_deep, gate_o, up_o, down_o1, down_o2 = lax.optimization_barrier(
-        (shared_both, shared_down, gate_o, up_o, down_o1, down_o2)
-    )
-    shared_wide = lax.all_gather(shared_both, "tp", axis=0, tiled=False)
-    shared_deep = lax.all_gather(shared_deep, "tp", axis=0, tiled=False)
+    both = jnp.concatenate([shared_gate, shared_up], axis=1)
+    both_l, both_r, deep_l, deep_r = right(both), left(both), right(shared_down), left(shared_down)
+    both_o, deep_o = right(both_l), left(deep_r)
 
     head_rows = attention(query_first, query_second, kv, lambda_head, head_gain)
 
@@ -368,10 +365,10 @@
     every = slice(None)
     shared = run_experts(
         normed,
-        (shared_wide, shared_deep),
-        tuple((0, i, every, pl.ds(0, part)) for i in range(ring)),
-        tuple((0, i, every, pl.ds(part, part)) for i in range(ring)),
-        tuple((1, i) for i in range(ring)),
+        (both, both_l, both_r, both_o, shared_down, deep_l, deep_r, deep_o),
+        tuple((i, every, pl.ds(0, part)) for i in range(ring)),
+        tuple((i, every, pl.ds(part, part)) for i in range(ring)),
+        tuple((ring + i,) for i in range(ring)),
         part,
         jnp.float32,
     )

time: 309 us -> 309 us (level)
  waiting for transfers between devices: 161 us -> 156 us
  starting transfers between devices: 58.7 us -> 62.8 us
    ppermute x5 -> x8, waiting for transfers between devices: 43.7 us -> 78.3 us  [right(): return lax.ppermute(value, 'tp', to_right)]
    all_to_all x1, waiting for transfers between devices: 72 us -> 43.6 us  [shards(): lax.all_to_all(outgoing, 'ep_0', split_axis=0, concat_axis=0, tiled=True)]
    ppermute x5 -> x8, waiting for transfers between devices: 43.5 us -> 33.3 us  [left(): return lax.ppermute(value, 'tp', to_left)]
    ppermute x5 -> x8, starting transfers between devices: 0.95 us -> 6.15 us  [right(): return lax.ppermute(value, 'tp', to_right)]
    unnamed x30 -> x49, local copies, waits for them, and re-layouts: 6.63 us -> 7.85 us
    ppermute x5 -> x8, starting transfers between devices: 17.1 us -> 16.3 us  [left(): return lax.ppermute(value, 'tp', to_left)]
  transfers between devices with their start and end apart: 19 -> 23, of which waited for: 6 -> 9; matrix products, arithmetic and copies ran while one was open for 1% -> 1% of each run, Pallas kernels for 19% -> 19%
where the time goes in v2:
time: 309 us; the launch traced here: 307 us
  waiting for transfers between devices  156 us (50%)
  starting transfers between devices  62.8 us (20%)
  Pallas kernels  58.8 us (19%)
  between operations  14.4 us (5%)
  local copies, waits for them, and re-layouts  8.79 us (3%)
  matrix products  3.75 us (1%)
    ppermute x8, waiting for transfers between devices, right(): return lax.ppermute(value, 'tp', to_right)  78.3 us
    all_to_all x1, waiting for transfers between devices, shards(): lax.all_to_all(outgoing, 'ep_0', split_axis=0, concat_axis=0, tiled=True)  43.6 us
    ppermute x8, waiting for transfers between devices, left(): return lax.ppermute(value, 'tp', to_left)  33.3 us
    pallas_call x1, Pallas kernels, attention(): pl.pallas_call(functools.partial(attention_kernel, steps, q_width // head...  33 us
    all_to_all x1, starting transfers between devices, shards(): lax.all_to_all(chunks, 'ep_0', split_axis=0, concat_axis=0, tiled=True)  24 us
    pallas_call x2, Pallas kernels, run_experts(): pl.pallas_call(functools.partial(experts_kernel, width, gates, ups, downs...  19.4 us
    ppermute x8, starting transfers between devices, left(): return lax.ppermute(value, 'tp', to_left)  16.3 us
    all_to_all x1, starting transfers between devices, shards(): lax.all_to_all(outgoing, 'ep_0', split_axis=0, concat_axis=0, tiled=True)  11.8 us
  transfers between devices with their start and end apart: 23, of which 9 were waited for; matrix products, arithmetic and copies ran while one was open for 1% of the time, Pallas kernels for 19%

profile of v2, /device:TPU:40, one launch (start us, length us, event | category | flops | bytes accessed | tf_op | source)
XLA Modules:
  0.0 306.6 jit_solution(11388308155497725350)
XLA Ops:
  7.2 0.1 all-gather.2.cloned.1.call-start
  7.2 1.8 pad_maximum_fusion
  9.1 0.1 all-gather.2.cloned.1.call-update
  9.1 0.1 collective-permute-start
  9.3 0.8 copy.31.own_ids_ref.ids_ref
  10.1 0.6 collective-permute-start.1
  10.7 0.9 collective-permute-done.1.other_ids_ref
  11.6 0.0 collective-permute-done.other_ref
  11.6 1.0 copy-done.1
  12.6 0.7 copy-done.4
  13.3 2.7 pack.1
  16.0 0.8 copy-done.7
  16.8 24.0 %all-to-all-start.1 = ((bf16[16,24,2048]{2,1,0:T(8,128)(2,1)}), bf16[16,24,2048]{2,1,0:T(8,128)(2,1)S(1)}, u32[]{:S(2)}, u32[]{:S(2)}) async-start(bf16[16,24,2048]{2,1,0:T(8,128)(2,1)} %bitcast.5), calls=%async_computation.1 | async-start | bytes 3145728 | tf_op jit(solution)/shard_map/all_to_all | solution.py:342
  40.8 1.8 collective-permute-start.8
  42.6 1.6 collective-permute-start.2
  44.2 1.6 collective-permute-start.6
  45.8 0.5 collective-permute-start.9
  46.3 1.9 collective-permute-start.3
  48.1 20.2 %collective-permute-done.8.refs_9_ = bf16[256,2048]{1,0:T(8,128)(2,1)S(1)} collective-permute-done((bf16[256,2048]{1,0:T(8,128)(2,1)}, bf16[256,2048]{1,0:T(8,128)(2,1)S(1)}, u32[]{:S(2)}, u32[]{:S(2)}) %collective-permute-start.8) | collective-permute-done | bytes 1048608 | tf_op jit(solution)/shard_map/ppermute | solution.py:318
  68.4 0.4 collective-permute-start.5
  68.8 22.0 %collective-permute-done.2.refs_1_ = bf16[2048,256]{1,0:T(8,128)(2,1)S(1)} collective-permute-done((bf16[2048,256]{1,0:T(8,128)(2,1)S(1)}, bf16[2048,256]{1,0:T(8,128)(2,1)S(1)}, u32[]{:S(2)}, u32[]{:S(2)}) %collective-permute-start.2) | collective-permute-done | bytes 1048608 | tf_op jit(solution)/shard_map/ppermute | solution.py:318
  90.8 0.4 collective-permute-start.4
  91.3 0.0 collective-permute-done.6.refs_6_
  91.3 2.8 collective-permute-start.7
  94.1 0.0 collective-permute-done.9.refs_10_
  94.2 0.1 collective-permute-start.10
  94.3 21.0 %collective-permute-done.3.refs_2_ = bf16[2048,256]{1,0:T(8,128)(2,1)S(1)} collective-permute-done((bf16[2048,256]{1,0:T(8,128)(2,1)S(1)}, bf16[2048,256]{1,0:T(8,128)(2,1)S(1)}, u32[]{:S(2)}, u32[]{:S(2)}) %collective-permute-start.3) | collective-permute-done | bytes 1048608 | tf_op jit(solution)/shard_map/ppermute | solution.py:321
  115.4 2.8 collective-permute-start.11
  118.2 0.0 collective-permute-done.5.refs_5_
  118.2 28.2 %collective-permute-done.10.refs_11_ = bf16[128,2048]{1,0:T(8,128)(2,1)S(1)} collective-permute-done((bf16[128,2048]{1,0:T(8,128)(2,1)S(1)}, bf16[128,2048]{1,0:T(8,128)(2,1)S(1)}, u32[]{:S(2)}, u32[]{:S(2)}) %collective-permute-start.10) | collective-permute-done | bytes 524320 | tf_op jit(solution)/shard_map/ppermute | solution.py:318
  146.3 1.3 collective-permute-done.11.refs_12_
  147.6 0.0 collective-permute-done.4.refs_3_
  147.7 1.0 copy-done.20
  148.7 0.0 collective-permute-done.7.refs_7_
  148.7 0.0 all-to-all-done.1
  148.7 0.0 copy-done.22
  148.8 1.1 copy-done.8
  149.9 13.4 %shard_map.185 = bf16[384,2048]{1,0:T(8,128)(2,1)} custom-call(bf16[384,2048]{1,0:T(8,128)(2,1)} %bitcast.20, bf16[2048,256]{1,0:T(8,128)(2,1)} %bitcast.24, bf16[2048,256]{1,0:T(8,128)(2,1)} %copy-done.15, bf16[2048,256]{1,0:T(8,128)(2,1)} %copy-done.17, bf16[2048,256]{1,0:T(8,128)(2,1)} %copy-done.20, bf16[2048,256]{1,0:T(8,128)(2,1)} %bitcast.29, ...), custom_call_target="tpu_custom_call" | custom-call | flops 14495514624 | bytes 12582912 | tf_op jit(solution)/shard_map/pallas_call | solution.py:228
  163.3 0.0 copy-start.10
  163.3 0.0 copy-start.13
  163.3 0.0 copy-start.2
  163.3 0.0 copy-start.3
  163.3 0.0 copy-start.5
  163.4 0.0 copy-start.6
  163.4 11.8 %all-to-all-start.2 = ((bf16[16,24,2048]{2,1,0:T(8,128)(2,1)}), bf16[16,24,2048]{2,1,0:T(8,128)(2,1)S(1)}, u32[]{:S(2)}, u32[]{:S(2)}) async-start(bf16[16,24,2048]{2,1,0:T(8,128)(2,1)} %bitcast.21), calls=%async_computation.2 | async-start | bytes 3145728 | tf_op jit(solution)/shard_map/all_to_all | solution.py:361
  175.2 0.9 constant_dynamic-update-slice_fusion.1
  176.1 0.8 constant_dynamic-update-slice_fusion.refs_0_
  176.9 1.3 collective-permute-start.13
  178.2 1.9 collective-permute-start.17
  180.2 1.6 collective-permute-start.14
  181.8 0.4 collective-permute-start.16
  182.2 0.1 copy.33.weights_ref
  182.3 11.0 %collective-permute-done.17.refs_6_ = bf16[128,2048]{1,0:T(8,128)(2,1)} collective-permute-done((bf16[128,2048]{1,0:T(8,128)(2,1)}, bf16[128,2048]{1,0:T(8,128)(2,1)}, u32[]{:S(2)}, u32[]{:S(2)}) %collective-permute-start.17) | collective-permute-done | bytes 524320 | tf_op jit(solution)/shard_map/ppermute | solution.py:321
  193.4 3.1 %collective-permute-start.18 = (bf16[128,2048]{1,0:T(8,128)(2,1)}, bf16[128,2048]{1,0:T(8,128)(2,1)}, u32[]{:S(2)}, u32[]{:S(2)}) collective-permute-start(bf16[128,2048]{1,0:T(8,128)(2,1)} %collective-permute-done.17.refs_6_), channel_id=1, source_target_pairs={{0,3},{1,0},{2,1},{3,2},{4,7},{5,4},{6,5},{7,6},{8,11},{9,8},{10,9... | collective-permute-start | bytes 1572872 | tf_op jit(solution)/shard_map/ppermute | solution.py:321
  196.5 7.9 %collective-permute-done.13.refs_1_ = bf16[2048,256]{1,0:T(8,128)(2,1)S(1)} collective-permute-done((bf16[2048,256]{1,0:T(8,128)(2,1)}, bf16[2048,256]{1,0:T(8,128)(2,1)S(1)}, u32[]{:S(2)}, u32[]{:S(2)}) %collective-permute-start.13) | collective-permute-done | bytes 1048608 | tf_op jit(solution)/shard_map/ppermute | solution.py:318
  204.4 0.1 collective-permute-start.15
  204.5 43.6 %all-to-all-done.2 = bf16[16,24,2048]{2,1,0:T(8,128)(2,1)S(1)} async-done(((bf16[16,24,2048]{2,1,0:T(8,128)(2,1)}), bf16[16,24,2048]{2,1,0:T(8,128)(2,1)S(1)}, u32[]{:S(2)}, u32[]{:S(2)}) %all-to-all-start.2) | async-done | bytes 1572896 | tf_op jit(solution)/shard_map/all_to_all | solution.py:361
  248.1 0.0 collective-permute-start.12
  248.2 33.0 %attention.1 = bf16[384,256]{1,0:T(8,128)(2,1)} custom-call(f32[2]{0:T(128)S(1)} %copy-done.5, f32[1,128]{1,0:T(1,128)S(1)} %bitcast.19, bf16[384,128]{1,0:T(8,128)(2,1)S(1)} %copy-done.2, bf16[384,128]{1,0:T(8,128)(2,1)S(1)} %copy-done.3, bf16[12288,512]{1,0:T(8,128)(2,1)} %all-gather.2.cloned.1.call-done.kv_ref), custom_call_target="tpu_custom_call" | custom-call | flops 28991029248 | bytes 12582912 | tf_op jit(solution)/shard_map/attention/pallas_call | solution.py:83
  281.1 3.7 %all-to-all-start = ((bf16[4,96,256]{2,1,0:T(8,128)(2,1)}), bf16[4,96,256]{2,1,0:T(8,128)(2,1)S(1)}, u32[]{:S(2)}, u32[]{:S(2)}) async-start(bf16[4,96,256]{2,1,0:T(8,128)(2,1)} %bitcast.1), calls=%async_computation | async-start | bytes 393216 | tf_op jit(solution)/shard_map/all_to_all | solution.py:375
  284.9 6.0 %shard_map.186.shared_ref = f32[128,2048]{1,0:T(8,128)} custom-call(bf16[128,2048]{1,0:T(8,128)(2,1)} %copy-done.7, bf16[2048,256]{1,0:T(8,128)(2,1)} %constant_dynamic-update-slice_fusion.refs_0_, bf16[2048,256]{1,0:T(8,128)(2,1)} %copy-done.18, bf16[2048,256]{1,0:T(8,128)(2,1)} %collective-permute-done.14.refs_2_, ...), custom_call_target="tpu_custom_call" | custom-call | flops 2415919104 | bytes 6291456 | tf_op jit(solution)/shard_map/pallas_call | solution.py:228
  290.9 1.2 copy-done
  292.1 3.8 %combine.1 = bf16[128,2048]{1,0:T(8,128)(2,1)} custom-call(s32[1]{0:T(128)} %bitcast.3.core_ref, bf16[384,2048]{1,0:T(8,128)(2,1)S(1)} %bitcast.17, bf16[384,2048]{1,0:T(8,128)(2,1)} %collective-permute-done.12.other_ref, s32[128,2]{1,0:T(8,128)S(1)} %copy.31.own_ids_ref.ids_ref, f32[128,2]{1,0:T(8,128)S(1)} %copy.33.weights_ref, f32[128,2048]{1,0:T(8,128)S(1)} %copy-done), custom_call_target="tpu_custom_call" | custom-call | flops 805306368 | bytes 3145728 | tf_op jit(solution)/shard_map/combine/pallas_call | solution.py:271
  295.9 3.8 %convolution_convert_fusion = bf16[96,2048]{1,0:T(8,128)(2,1)} fusion(bf16[96,1024]{1,0:T(8,128)(2,1)S(1)} %bitcast.22, bf16[1024,2048]{1,0:T(8,128)(2,1)} %param.25), kind=kOutput, calls=%fused_computation | convolution fusion | flops 402849792 | bytes 4784128 | tf_op jit(solution)/shard_map/dot_general | solution.py:376
  (43 shorter events, 0.2 us)
Async XLA Ops:
  7.2 240.9 %all-gather.2.cloned.1.call-start = ((), (), s32[]{:S(2)}) async-start(), calls=%async_computation.3 | async-start | bytes 12976128 | tf_op jit(solution)/shard_map/all_gather | solution.py:334
  9.1 2.4 collective-permute-start
  10.1 1.5 collective-permute-start.1
  11.6 1.0 copy-start.1
  12.6 0.7 copy-start.4
  13.3 29.2 %copy-start.14 = (bf16[1,2048,256]{2,1,0:T(8,128)(2,1)S(1)}, bf16[1,2048,256]{2,1,0:T(8,128)(2,1)}, u32[]{:S(2)}) copy-start(bf16[1,2048,256]{2,1,0:T(8,128)(2,1)} %param.30) | copy-start | bytes 3145732
  16.0 0.8 copy-start.7
  16.8 131.9 %all-to-all-start.1 = ((bf16[16,24,2048]{2,1,0:T(8,128)(2,1)}), bf16[16,24,2048]{2,1,0:T(8,128)(2,1)S(1)}, u32[]{:S(2)}, u32[]{:S(2)}) async-start(bf16[16,24,2048]{2,1,0:T(8,128)(2,1)} %bitcast.5), calls=%async_computation.1 | async-start | bytes 3145728 | tf_op jit(solution)/shard_map/all_to_all | solution.py:342
  40.8 27.6 %collective-permute-start.8 = (bf16[256,2048]{1,0:T(8,128)(2,1)}, bf16[256,2048]{1,0:T(8,128)(2,1)S(1)}, u32[]{:S(2)}, u32[]{:S(2)}) collective-permute-start(bf16[256,2048]{1,0:T(8,128)(2,1)} %bitcast.30), channel_id=1, source_target_pairs={{0,1},{1,2},{2,3},{3,0},{4,5},{5,6},{6,7},{7,4},{8,9},{9,10},{10,1... | collective-permute-start | bytes 3145736 | tf_op jit(solution)/shard_map/ppermute | solution.py:318
  42.6 48.3 %collective-permute-start.2 = (bf16[2048,256]{1,0:T(8,128)(2,1)S(1)}, bf16[2048,256]{1,0:T(8,128)(2,1)S(1)}, u32[]{:S(2)}, u32[]{:S(2)}) collective-permute-start(bf16[2048,256]{1,0:T(8,128)(2,1)S(1)} %bitcast.25), channel_id=1, source_target_pairs={{0,1},{1,2},{2,3},{3,0},{4,5},{5,6},{6,7},{7,4},{8,9},{9,10},{10,1... | collective-permute-start | bytes 3145736 | tf_op jit(solution)/shard_map/ppermute | solution.py:318
  44.2 47.1 %collective-permute-start.6 = (bf16[2048,256]{1,0:T(8,128)(2,1)}, bf16[2048,256]{1,0:T(8,128)(2,1)S(1)}, u32[]{:S(2)}, u32[]{:S(2)}) collective-permute-start(bf16[2048,256]{1,0:T(8,128)(2,1)} %bitcast.27), channel_id=1, source_target_pairs={{0,3},{1,0},{2,1},{3,2},{4,7},{5,4},{6,5},{7,6},{8,11},{9,8},{10,9... | collective-permute-start | bytes 3145736 | tf_op jit(solution)/shard_map/ppermute | solution.py:321
  45.8 48.3 %collective-permute-start.9 = (bf16[256,2048]{1,0:T(8,128)(2,1)}, bf16[256,2048]{1,0:T(8,128)(2,1)S(1)}, u32[]{:S(2)}, u32[]{:S(2)}) collective-permute-start(bf16[256,2048]{1,0:T(8,128)(2,1)} %bitcast.31), channel_id=1, source_target_pairs={{0,3},{1,0},{2,1},{3,2},{4,7},{5,4},{6,5},{7,6},{8,11},{9,8},{10,9... | collective-permute-start | bytes 3145736 | tf_op jit(solution)/shard_map/ppermute | solution.py:321
  46.3 69.1 %collective-permute-start.3 = (bf16[2048,256]{1,0:T(8,128)(2,1)S(1)}, bf16[2048,256]{1,0:T(8,128)(2,1)S(1)}, u32[]{:S(2)}, u32[]{:S(2)}) collective-permute-start(bf16[2048,256]{1,0:T(8,128)(2,1)S(1)} %bitcast.26), channel_id=1, source_target_pairs={{0,3},{1,0},{2,1},{3,2},{4,7},{5,4},{6,5},{7,6},{8,11},{9,8},{10,9... | collective-permute-start | bytes 3145736 | tf_op jit(solution)/shard_map/ppermute | solution.py:321
  68.4 25.8 %copy-start.11 = (bf16[256,2048]{1,0:T(8,128)(2,1)}, bf16[256,2048]{1,0:T(8,128)(2,1)S(1)}, u32[]{:S(2)}) copy-start(bf16[256,2048]{1,0:T(8,128)(2,1)S(1)} %collective-permute-done.8.refs_9_) | copy-start | bytes 3145732
  68.4 49.8 %collective-permute-start.5 = (bf16[2048,256]{1,0:T(8,128)(2,1)}, bf16[2048,256]{1,0:T(8,128)(2,1)S(1)}, u32[]{:S(2)}, u32[]{:S(2)}) collective-permute-start(bf16[2048,256]{1,0:T(8,128)(2,1)} %bitcast.28), channel_id=1, source_target_pairs={{0,1},{1,2},{2,3},{3,0},{4,5},{5,6},{6,7},{7,4},{8,9},{9,10},{10,1... | collective-permute-start | bytes 3145736 | tf_op jit(solution)/shard_map/ppermute | solution.py:318
  90.8 56.8 %copy-start.15 = (bf16[2048,256]{1,0:T(8,128)(2,1)}, bf16[2048,256]{1,0:T(8,128)(2,1)S(1)}, u32[]{:S(2)}) copy-start(bf16[2048,256]{1,0:T(8,128)(2,1)S(1)} %collective-permute-done.2.refs_1_) | copy-start | bytes 3145732
  90.8 56.8 %collective-permute-start.4 = (bf16[2048,256]{1,0:T(8,128)(2,1)S(1)}, bf16[2048,256]{1,0:T(8,128)(2,1)S(1)}, u32[]{:S(2)}, u32[]{:S(2)}) collective-permute-start(bf16[2048,256]{1,0:T(8,128)(2,1)S(1)} %collective-permute-done.2.refs_1_), channel_id=1, source_target_pairs={{0,1},{1,2},{2,3},{3,0},{4,5},{5,6},{6,7},{7,4},{8,9},{9,10},{10,1... | collective-permute-start | bytes 3145736 | tf_op jit(solution)/shard_map/ppermute | solution.py:318
  91.3 56.3 %copy-start.16 = (bf16[2048,256]{1,0:T(8,128)(2,1)}, bf16[2048,256]{1,0:T(8,128)(2,1)S(1)}, u32[]{:S(2)}) copy-start(bf16[2048,256]{1,0:T(8,128)(2,1)S(1)} %collective-permute-done.6.refs_6_) | copy-start | bytes 3145732
  91.3 57.4 %collective-permute-start.7 = (bf16[2048,256]{1,0:T(8,128)(2,1)S(1)}, bf16[2048,256]{1,0:T(8,128)(2,1)}, u32[]{:S(2)}, u32[]{:S(2)}) collective-permute-start(bf16[2048,256]{1,0:T(8,128)(2,1)S(1)} %collective-permute-done.6.refs_6_), channel_id=1, source_target_pairs={{0,3},{1,0},{2,1},{3,2},{4,7},{5,4},{6,5},{7,6},{8,11},{9,8},{10,9... | collective-permute-start | bytes 3145736 | tf_op jit(solution)/shard_map/ppermute | solution.py:321
  94.1 53.5 %copy-start.12 = (bf16[256,2048]{1,0:T(8,128)(2,1)}, bf16[256,2048]{1,0:T(8,128)(2,1)S(1)}, u32[]{:S(2)}) copy-start(bf16[256,2048]{1,0:T(8,128)(2,1)S(1)} %collective-permute-done.9.refs_10_) | copy-start | bytes 3145732
  94.2 52.2 %collective-permute-start.10 = (bf16[128,2048]{1,0:T(8,128)(2,1)S(1)}, bf16[128,2048]{1,0:T(8,128)(2,1)S(1)}, u32[]{:S(2)}, u32[]{:S(2)}) collective-permute-start(bf16[128,2048]{1,0:T(8,128)(2,1)S(1)} %slice.8), channel_id=1, source_target_pairs={{0,1},{1,2},{2,3},{3,0},{4,5},{5,6},{6,7},{7,4},{8,9},{9,10},{10,1... | collective-permute-start | bytes 1572872 | tf_op jit(solution)/shard_map/ppermute | solution.py:318
  115.4 32.3 %copy-start.17 = (bf16[2048,256]{1,0:T(8,128)(2,1)}, bf16[2048,256]{1,0:T(8,128)(2,1)S(1)}, u32[]{:S(2)}) copy-start(bf16[2048,256]{1,0:T(8,128)(2,1)S(1)} %collective-permute-done.3.refs_2_) | copy-start | bytes 3145732
  115.4 32.2 %collective-permute-start.11 = (bf16[128,2048]{1,0:T(8,128)(2,1)S(1)}, bf16[128,2048]{1,0:T(8,128)(2,1)S(1)}, u32[]{:S(2)}, u32[]{:S(2)}) collective-permute-start(bf16[128,2048]{1,0:T(8,128)(2,1)S(1)} %slice.9), channel_id=1, source_target_pairs={{0,3},{1,0},{2,1},{3,2},{4,7},{5,4},{6,5},{7,6},{8,11},{9,8},{10,9... | collective-permute-start | bytes 1572872 | tf_op jit(solution)/shard_map/ppermute | solution.py:321
  118.2 29.5 %copy-start.19 = (bf16[2048,256]{1,0:T(8,128)(2,1)}, bf16[2048,256]{1,0:T(8,128)(2,1)S(1)}, u32[]{:S(2)}) copy-start(bf16[2048,256]{1,0:T(8,128)(2,1)S(1)} %collective-permute-done.5.refs_5_) | copy-start | bytes 3145732
  146.3 1.3 copy-start.21
  147.6 1.2 copy-start.22
  147.7 1.0 copy-start.20
  148.7 1.2 copy-start.8
  149.9 25.3 %copy-start.9 = (bf16[2048,128]{1,0:T(8,128)(2,1)S(1)}, bf16[2048,128]{1,0:T(8,128)(2,1)}, u32[]{:S(2)}) copy-start(bf16[2048,128]{1,0:T(8,128)(2,1)} %param.33) | copy-start | bytes 1572868
  163.3 12.8 %copy-start.10 = (bf16[2048,128]{1,0:T(8,128)(2,1)S(1)}, bf16[2048,128]{1,0:T(8,128)(2,1)}, u32[]{:S(2)}) copy-start(bf16[2048,128]{1,0:T(8,128)(2,1)} %param.34) | copy-start | bytes 1572868
  163.3 18.9 %copy-start.13 = (f32[128,2]{0,1:T(2,128)S(1)}, f32[128,2]{0,1:T(2,128)}, u32[]{:S(2)}) copy-start(f32[128,2]{0,1:T(2,128)} %param.29) | copy-start | bytes 3076
  163.3 84.8 %copy-start.2 = (bf16[384,128]{1,0:T(8,128)(2,1)S(1)}, bf16[384,128]{1,0:T(8,128)(2,1)}, u32[]{:S(2)}) copy-start(bf16[384,128]{1,0:T(8,128)(2,1)} %q1_ref.1) | copy-start | bytes 294916
  163.3 84.8 %copy-start.3 = (bf16[384,128]{1,0:T(8,128)(2,1)S(1)}, bf16[384,128]{1,0:T(8,128)(2,1)}, u32[]{:S(2)}) copy-start(bf16[384,128]{1,0:T(8,128)(2,1)} %q2_ref.1) | copy-start | bytes 294916
  163.3 84.8 %copy-start.5 = (f32[2]{0:T(128)S(1)}, f32[2]{0:T(128)}, u32[]{:S(2)}) copy-start(f32[2]{0:T(128)} %lam_ref.1) | copy-start | bytes 28
  163.4 84.8 %copy-start.6 = (f32[128]{0:T(128)S(1)}, f32[128]{0:T(128)}, u32[]{:S(2)}) copy-start(f32[128]{0:T(128)} %param.24) | copy-start | bytes 1540
  163.4 84.7 %all-to-all-start.2 = ((bf16[16,24,2048]{2,1,0:T(8,128)(2,1)}), bf16[16,24,2048]{2,1,0:T(8,128)(2,1)S(1)}, u32[]{:S(2)}, u32[]{:S(2)}) async-start(bf16[16,24,2048]{2,1,0:T(8,128)(2,1)} %bitcast.21), calls=%async_computation.2 | async-start | bytes 3145728 | tf_op jit(solution)/shard_map/all_to_all | solution.py:361
  176.9 27.4 %collective-permute-start.13 = (bf16[2048,256]{1,0:T(8,128)(2,1)}, bf16[2048,256]{1,0:T(8,128)(2,1)S(1)}, u32[]{:S(2)}, u32[]{:S(2)}) collective-permute-start(bf16[2048,256]{1,0:T(8,128)(2,1)} %constant_dynamic-update-slice_fusion.refs_0_), channel_id=1, source_target_pairs={{0,1},{1,2},{2,3},{3,0},{4,5},{5,6},{6,7},{7,4},{8,9},{9,10},{10,1... | collective-permute-start | bytes 3145736 | tf_op jit(solution)/shard_map/ppermute | solution.py:318
  178.2 15.1 %collective-permute-start.17 = (bf16[128,2048]{1,0:T(8,128)(2,1)}, bf16[128,2048]{1,0:T(8,128)(2,1)}, u32[]{:S(2)}, u32[]{:S(2)}) collective-permute-start(bf16[128,2048]{1,0:T(8,128)(2,1)} %refs_4_.1), channel_id=1, source_target_pairs={{0,3},{1,0},{2,1},{3,2},{4,7},{5,4},{6,5},{7,6},{8,11},{9,8},{10,9... | collective-permute-start | bytes 1572872 | tf_op jit(solution)/shard_map/ppermute | solution.py:321
  180.2 104.7 %collective-permute-start.14 = (bf16[2048,256]{1,0:T(8,128)(2,1)}, bf16[2048,256]{1,0:T(8,128)(2,1)}, u32[]{:S(2)}, u32[]{:S(2)}) collective-permute-start(bf16[2048,256]{1,0:T(8,128)(2,1)} %constant_dynamic-update-slice_fusion.refs_0_), channel_id=1, source_target_pairs={{0,3},{1,0},{2,1},{3,2},{4,7},{5,4},{6,5},{7,6},{8,11},{9,8},{10,9... | collective-permute-start | bytes 3145736 | tf_op jit(solution)/shard_map/ppermute | solution.py:321
  181.8 103.0 %collective-permute-start.16 = (bf16[128,2048]{1,0:T(8,128)(2,1)}, bf16[128,2048]{1,0:T(8,128)(2,1)}, u32[]{:S(2)}, u32[]{:S(2)}) collective-permute-start(bf16[128,2048]{1,0:T(8,128)(2,1)} %refs_4_.1), channel_id=1, source_target_pairs={{0,1},{1,2},{2,3},{3,0},{4,5},{5,6},{6,7},{7,4},{8,9},{9,10},{10,1... | collective-permute-start | bytes 1572872 | tf_op jit(solution)/shard_map/ppermute | solution.py:318
  193.4 91.5 %collective-permute-start.18 = (bf16[128,2048]{1,0:T(8,128)(2,1)}, bf16[128,2048]{1,0:T(8,128)(2,1)}, u32[]{:S(2)}, u32[]{:S(2)}) collective-permute-start(bf16[128,2048]{1,0:T(8,128)(2,1)} %collective-permute-done.17.refs_6_), channel_id=1, source_target_pairs={{0,3},{1,0},{2,1},{3,2},{4,7},{5,4},{6,5},{7,6},{8,11},{9,8},{10,9... | collective-permute-start | bytes 1572872 | tf_op jit(solution)/shard_map/ppermute | solution.py:321
  204.4 76.7 %copy-start.18 = (bf16[2048,256]{1,0:T(8,128)(2,1)}, bf16[2048,256]{1,0:T(8,128)(2,1)S(1)}, u32[]{:S(2)}) copy-start(bf16[2048,256]{1,0:T(8,128)(2,1)S(1)} %collective-permute-done.13.refs_1_) | copy-start | bytes 3145732
  204.4 80.5 %collective-permute-start.15 = (bf16[2048,256]{1,0:T(8,128)(2,1)S(1)}, bf16[2048,256]{1,0:T(8,128)(2,1)}, u32[]{:S(2)}, u32[]{:S(2)}) collective-permute-start(bf16[2048,256]{1,0:T(8,128)(2,1)S(1)} %collective-permute-done.13.refs_1_), channel_id=1, source_target_pairs={{0,1},{1,2},{2,3},{3,0},{4,5},{5,6},{6,7},{7,4},{8,9},{9,10},{10,1... | collective-permute-start | bytes 3145736 | tf_op jit(solution)/shard_map/ppermute | solution.py:318
  248.1 42.7 %collective-permute-start.12 = (bf16[384,2048]{1,0:T(8,128)(2,1)S(1)}, bf16[384,2048]{1,0:T(8,128)(2,1)}, u32[]{:S(2)}, u32[]{:S(2)}) collective-permute-start(bf16[384,2048]{1,0:T(8,128)(2,1)S(1)} %bitcast.16), channel_id=1, source_target_pairs={{0,4},{4,0},{1,5},{5,1},{2,6},{6,2},{3,7},{7,3},{8,12},{12,8},{9,1... | collective-permute-start | bytes 4718600 | tf_op jit(solution)/shard_map/ppermute | solution.py:315
  281.1 14.8 %all-to-all-start = ((bf16[4,96,256]{2,1,0:T(8,128)(2,1)}), bf16[4,96,256]{2,1,0:T(8,128)(2,1)S(1)}, u32[]{:S(2)}, u32[]{:S(2)}) async-start(bf16[4,96,256]{2,1,0:T(8,128)(2,1)} %bitcast.1), calls=%async_computation | async-start | bytes 393216 | tf_op jit(solution)/shard_map/all_to_all | solution.py:375
  290.9 1.2 copy-start
Sparse Core Ops, SparseCore 0:
  10.4 165.8 all-gather.1
